TPU v7x, 32 devices: a whole 2x2x4 slice. The times are simulated.
32 devices in a mesh: fs: 8 (over z, y), tp: 4 (over x, core).
Axes of the slice: x: 2, y: 2, z: 4, core: 2. Of those that a mesh axis runs over, the one named last changes fastest.
Arguments:
- hidden_states: bfloat16 [2048, 2048], P('tp', 'fs'), may hold values from -6 to 6
- norm_gain: float32 [2048], P('fs'), may hold values from 0.1 to 1.9
- gate_master: float32 [8, 2048, 7168], P(None, 'fs', 'tp'), may hold values from -0.125 to 0.125
- up_master: float32 [8, 2048, 7168], P(None, 'fs', 'tp'), may hold values from -0.125 to 0.125
- down_master: float32 [8, 2048, 7168], P(None, 'fs', 'tp'), may hold values from -0.0625 to 0.0625
- expert_ids: int32 [2048, 2], P('tp'), may hold values from 0 to 7, all different within a row; in each aligned block of 512 rows (0 to 511, 512 to 1023, ...) at most 256 rows name the same one
- route_logits: float32 [2048, 2], P('tp'), may hold values from -6 to 6
Outputs:
- gate_serve: bfloat16 [8, 2048, 7168], P('tp', None, 'fs')
- up_serve: bfloat16 [8, 2048, 7168], P('tp', None, 'fs')
- down_serve: bfloat16 [8, 2048, 7168], P('tp', None, 'fs')
- combined: bfloat16 [2048, 2048], P('tp', 'fs')
Inputs may be any that keep to these rules, and one draw needn't show every extreme that they name: `expert_ids`: the 2 entries of a row differ. Among the rows of one index of tp (aligned blocks of 512 rows) no expert is named more than 256 times, and in some blocks one expert is named exactly 256 times.
All inputs are finite; a program needn't handle non-finite values.
Results may differ from a plain program's by a relative error of at most 0.018.
Values may be sent and summed in bfloat16 or wider, within the bound.
A program may use at most 192 MiB of HBM per device.

v0:
```python
import functools

import jax
import jax.numpy as jnp
from jax import lax
from jax.experimental import pallas as pl
from jax.experimental.pallas import tpu as pltpu
from jax.sharding import PartitionSpec as P

EPSILON = 1e-06
SLOTS = 4
MESH = pl.DeviceIdType.MESH


def exchange_kernel(
    groups, row_groups, expert, chunks, gain_ref, gate_ref, up_ref, down_ref, dep_ref,
    gate_out, up_out, down_out, stage, cast, landed, load_sem,
    send_a, recv_a, send_b, recv_b,
):
    me = lax.axis_index("tp")
    row = lax.axis_index("fs")
    blocks = row_groups // groups
    masters = (gate_ref, up_ref, down_ref)
    outs = (gate_out, up_out, down_out)
    local_count = gate_ref.shape[0] // groups
    rows, columns = gate_ref.shape[1:]
    height = rows // chunks
    width = columns // blocks

    barrier = pltpu.get_barrier_semaphore()
    for step in range(1, groups):
        pl.semaphore_signal(
            barrier, inc=1, device_id={"tp": lax.rem(me + step, groups)}, device_id_type=MESH
        )
    for step in range(1, row_groups):
        pl.semaphore_signal(
            barrier, inc=1, device_id={"fs": lax.rem(row + step, row_groups)}, device_id_type=MESH
        )
    order = [groups // 2] + [s for s in range(1, groups) if s != groups // 2] + [0]
    units = [(w, c) for w in range(len(masters)) for c in range(chunks)]
    jobs = [(u, s) for u in range(len(units)) for s in order]

    def load(n):
        u, s = jobs[n]
        w, c = units[u]
        number = lax.rem(me + s, groups) * local_count + expert
        return pltpu.make_async_copy(
            masters[w].at[number, pl.ds(c * height, height)],
            stage.at[n % SLOTS],
            load_sem.at[n % SLOTS],
        )

    for n in range(SLOTS):
        load(n).start()
    pl.semaphore_wait(barrier, groups - 1 + row_groups - 1)

    def first(u, s):
        return pltpu.make_async_remote_copy(
            src_ref=cast.at[u, s],
            dst_ref=landed.at[u, s - 1],
            send_sem=send_a.at[u, s - 1],
            recv_sem=recv_a.at[u, s - 1],
            device_id={"tp": lax.rem(me + s, groups)},
            device_id_type=MESH,
        )

    def place(u, source):
        w, c = units[u]
        start = pl.multiple_of(source * rows + c * height, height)
        return outs[w].at[pl.ds(start, height)]

    def second(u, s, b):
        held = cast.at[u, 0] if s == 0 else landed.at[u, s - 1]
        goal = lax.rem(me + groups - s, groups) * blocks + b
        piece = held.at[:, pl.ds(b * width, width)]
        remote = lambda: pltpu.make_async_remote_copy(
            src_ref=piece,
            dst_ref=place(u, row),
            send_sem=send_b.at[u, s * blocks + b],
            recv_sem=recv_b.at[u, row],
            device_id={"fs": goal},
            device_id_type=MESH,
        )
        local = lambda: pltpu.make_async_copy(piece, place(u, row), recv_b.at[u, row])
        return goal, remote, local

    def pass_on(u, s):
        for b in range(blocks):
            goal, remote, local = second(u, s, b)

            @pl.when(goal != row)
            def _():
                remote().start()

            @pl.when(goal == row)
            def _():
                local().start()

    def forward(u):
        for s in sorted(range(1, groups), key=lambda s: s == groups // 2):
            first(u, s).wait_recv()
            pass_on(u, s)

    strip = 16
    for n, (u, s) in enumerate(jobs):
        w, c = units[u]
        load(n).wait()
        slot = n % SLOTS

        def convert(i, carry):
            at = pl.ds(pl.multiple_of(i * strip, strip), strip)
            value = stage[slot, at, :]
            if w < 2:
                gain = gain_ref[pl.ds(pl.multiple_of(c * height + i * strip, strip), strip), :]
                value = value * gain
            cast[u, s, at, :] = value.astype(jnp.bfloat16)
            return carry

        lax.fori_loop(0, height // strip, convert, 0)
        if n + SLOTS < len(jobs):
            load(n + SLOTS).start()
        if s == 0:
            pass_on(u, 0)
            if u >= 1:
                forward(u - 1)
        else:
            first(u, s).start()
    forward(len(units) - 1)
    for u in range(len(units)):
        for s in range(groups):
            if s:
                first(u, s).wait_send()
            for b in range(blocks):
                goal, remote, local = second(u, s, b)

                @pl.when(goal != row)
                def _():
                    remote().wait_send()
        for source in range(row_groups):
            pltpu.make_async_copy(
                cast.at[u, 0, :, pl.ds(0, width)], place(u, source), recv_b.at[u, source]
            ).wait()


def exchange(gain, gate, up, down, dep, expert, collective):
    groups = lax.axis_size("tp")
    row_groups = lax.axis_size("fs")
    experts, rows, columns = gate.shape
    blocks = row_groups // groups
    width = columns // blocks
    chunks = 2
    units = 3 * chunks
    height = rows // chunks
    out = jax.ShapeDtypeStruct((rows * row_groups, width), jnp.bfloat16)
    hbm = pl.BlockSpec(memory_space=pl.ANY)
    sent = 3 * rows * columns * 2 * groups
    return pl.pallas_call(
        functools.partial(exchange_kernel, groups, row_groups, expert, chunks),
        out_shape=(out, out, out),
        in_specs=[pl.BlockSpec(memory_space=pltpu.VMEM), hbm, hbm, hbm, hbm],
        out_specs=(hbm, hbm, hbm),
        scratch_shapes=[
            pltpu.VMEM((SLOTS, height, columns), jnp.float32),
            pltpu.VMEM((units, groups, height, columns), jnp.bfloat16),
            pltpu.VMEM((units, groups - 1, height, columns), jnp.bfloat16),
            pltpu.SemaphoreType.DMA((SLOTS,)),
            pltpu.SemaphoreType.DMA((units, groups - 1)),
            pltpu.SemaphoreType.DMA((units, groups - 1)),
            pltpu.SemaphoreType.DMA((units, row_groups)),
            pltpu.SemaphoreType.DMA((units, row_groups)),
        ],
        compiler_params=pltpu.CompilerParams(
            collective_id=collective, has_side_effects=True, vmem_limit_bytes=44 * 1024 * 1024
        ),
        cost_estimate=pl.CostEstimate(
            flops=rows * columns, bytes_accessed=32 * sent, transcendentals=0
        ),
    )(gain, gate, up, down, dep)


def serve_kernel(
    groups, row_groups, expert, chunks, gain_ref, gate_ref, up_ref, down_ref, all_ref, spot_ref,
    gate_first, up_first, down_first,
    gate_out, up_out, down_out, early_out, partial_out,
    stage, cast, landed, raw, rows_in, gate_w, up_w, down_w, act, partial, pair, summed, far, total,
    load_sem, send_a, recv_a, send_b, recv_b, raw_sem, weight_sem, keep_sem,
    send_c, recv_c, send_d, recv_d, send_e, recv_e, last_sem,
):
    me = lax.axis_index("tp")
    row = lax.axis_index("fs")
    blocks = row_groups // groups
    masters = (gate_ref, up_ref, down_ref)
    outs = (gate_out, up_out, down_out)
    firsts = (gate_first, up_first, down_first)
    held_w = (gate_w, up_w, down_w)
    local_count = gate_ref.shape[0] // groups
    rows, columns = gate_ref.shape[1:]
    height = rows // chunks
    width = columns // blocks
    tokens, model_width = raw.shape
    capacity = tokens // 2
    side = lax.rem(row, 2)
    mate = row + 1 - 2 * side
    stack = row_groups // 2
    level = row // 2
    strip = 16

    barrier = pltpu.get_barrier_semaphore()
    for step in range(1, groups):
        pl.semaphore_signal(
            barrier, inc=1, device_id={"tp": lax.rem(me + step, groups)}, device_id_type=MESH
        )
    for step in range(1, row_groups):
        pl.semaphore_signal(
            barrier, inc=1, device_id={"fs": lax.rem(row + step, row_groups)}, device_id_type=MESH
        )
    order = [groups // 2] + [s for s in range(1, groups) if s != groups // 2] + [0]
    units = [(w, c) for w in range(len(masters)) for c in range(chunks)]
    jobs = [(u, s) for u in range(len(units)) for s in order]

    def load(n):
        u, s = jobs[n]
        w, c = units[u]
        number = lax.rem(me + s, groups) * local_count + expert
        return pltpu.make_async_copy(
            masters[w].at[number, pl.ds(c * height, height)],
            stage.at[n % SLOTS],
            load_sem.at[n % SLOTS],
        )

    for n in range(SLOTS):
        load(n).start()
    pl.semaphore_wait(barrier, groups - 1 + row_groups - 1)

    def first(u, s):
        return pltpu.make_async_remote_copy(
            src_ref=cast.at[u, s],
            dst_ref=landed.at[u, s - 1],
            send_sem=send_a.at[u, s - 1],
            recv_sem=recv_a.at[u, s - 1],
            device_id={"tp": lax.rem(me + s, groups)},
            device_id_type=MESH,
        )

    def place(u, source):
        w, c = units[u]
        start = pl.multiple_of(source * rows + c * height, height)
        return outs[w].at[expert, pl.ds(start, height)]

    def second(u, s, b):
        held = cast.at[u, 0] if s == 0 else landed.at[u, s - 1]
        goal = lax.rem(me + groups - s, groups) * blocks + b
        piece = held.at[:, pl.ds(b * width, width)]
        remote = lambda: pltpu.make_async_remote_copy(
            src_ref=piece,
            dst_ref=place(u, row),
            send_sem=send_b.at[u, s * blocks + b],
            recv_sem=recv_b.at[u, row],
            device_id={"fs": goal},
            device_id_type=MESH,
        )
        local = lambda: pltpu.make_async_copy(piece, place(u, row), recv_b.at[u, row])
        return goal, remote, local

    def pass_on(u, s):
        for b in range(blocks):
            goal, remote, local = second(u, s, b)

            @pl.when(goal != row)
            def _():
                remote().start()

            @pl.when(goal == row)
            def _():
                local().start()

    def forward(u):
        for s in sorted(range(1, groups), key=lambda s: s == groups // 2):
            first(u, s).wait_recv()
            pass_on(u, s)

    def arrived(u):
        for source in range(row_groups):
            pltpu.make_async_copy(
                cast.at[u, 0, :, pl.ds(0, width)], place(u, source), recv_b.at[u, source]
            ).wait()

    def pack(j):
        def one(g, carry):
            copies = [
                pltpu.make_async_copy(
                    all_ref.at[f, g, pl.ds(0, tokens)],
                    raw.at[:, pl.ds(f * (model_width // row_groups), model_width // row_groups)],
                    raw_sem.at[f],
                )
                for f in range(row_groups)
            ]
            for copy in copies:
                copy.start()
            for copy in copies:
                copy.wait()
            spot = spot_ref[pl.ds(j * groups + g, 1), :]
            slot = lax.broadcasted_iota(jnp.int32, (capacity, tokens), 0)
            table = jnp.where(slot == spot, 1.0, 0.0).astype(jnp.bfloat16)
            packed = jnp.dot(table, raw[...], preferred_element_type=jnp.float32)
            mean = jnp.mean(packed * packed, axis=1, keepdims=True)
            at = pl.ds(pl.multiple_of(g * capacity, capacity), capacity)
            rows_in[at, :] = (packed * lax.rsqrt(mean + EPSILON)).astype(jnp.bfloat16)
            return carry

        lax.fori_loop(0, groups, one, 0)

    def hidden():
        def one(t, carry):
            at = pl.ds(pl.multiple_of(t * capacity, capacity), capacity)
            value = rows_in[at, :]
            gate_pre = jnp.dot(value, gate_w[...], preferred_element_type=jnp.float32)
            up_pre = jnp.dot(value, up_w[...], preferred_element_type=jnp.float32)
            act[at, :] = (gate_pre / (1.0 + jnp.exp(-gate_pre)) * up_pre).astype(jnp.bfloat16)
            return carry

        lax.fori_loop(0, groups, one, 0)

    def lower():
        def one(r, carry):
            at = pl.ds(pl.multiple_of(r * rows, rows), rows)
            partial[at, :] = lax.dot_general(
                down_w[at, :], act[...], (((1,), (1,)), ((), ())), preferred_element_type=jnp.float32
            ).astype(jnp.bfloat16)
            return carry

        lax.fori_loop(0, row_groups, one, 0)

    def fetch(w, j):
        source = firsts[w] if j == 0 else outs[w].at[j]
        return pltpu.make_async_copy(source, held_w[w], weight_sem.at[w])

    def keep(w):
        return pltpu.make_async_copy(held_w[w], outs[w].at[0], keep_sem.at[w])

    levels = [stack // 2] + [k for k in range(1, stack) if k != stack // 2] + [0]

    def rows_of(k, which):
        return (lax.rem(level + k, stack) * 2 + which) * rows

    def across(k):
        return pltpu.make_async_remote_copy(
            src_ref=partial.at[pl.ds(pl.multiple_of(rows_of(k, 1 - side), rows), rows)],
            dst_ref=pair.at[k],
            send_sem=send_c.at[k],
            recv_sem=recv_c.at[k],
            device_id={"fs": mate},
            device_id_type=MESH,
        )

    def along(k):
        return pltpu.make_async_remote_copy(
            src_ref=summed.at[k - 1],
            dst_ref=far.at[k - 1],
            send_sem=send_d.at[k - 1],
            recv_sem=recv_d.at[k - 1],
            device_id={"fs": lax.rem(level + k, stack) * 2 + side},
            device_id_type=MESH,
        )

    def back(s):
        goal = lax.rem(me + s, groups)
        return pltpu.make_async_remote_copy(
            src_ref=total.at[:, pl.ds(pl.multiple_of(goal * capacity, capacity), capacity)],
            dst_ref=early_out.at[me],
            send_sem=send_e.at[s - 1],
            recv_sem=recv_e.at[s - 1],
            device_id={"tp": goal},
            device_id_type=MESH,
        )

    kept = pltpu.make_async_copy(
        total.at[:, pl.ds(pl.multiple_of(me * capacity, capacity), capacity)],
        early_out.at[me],
        last_sem.at[0],
    )

    def own_sum(k, i):
        at = pl.ds(pl.multiple_of(i * strip, strip), strip)
        mine = pl.ds(pl.multiple_of(rows_of(k, side) + i * strip, strip), strip)
        return at, partial[mine, :].astype(jnp.float32) + pair[k, at, :].astype(jnp.float32)

    def after_0():
        for w in range(len(masters)):
            fetch(w, 0).start()
        pack(0)

    def after_1():
        for w in range(2):
            fetch(w, 0).wait()
            keep(w).start()
        hidden()

    def after_2():
        fetch(2, 0).wait()
        keep(2).start()
        lower()
        for k in levels:
            across(k).start()

    def after_3():
        for k in levels:
            across(k).wait_recv()
            if k:

                def add(i, carry):
                    at, both = own_sum(k, i)
                    summed[k - 1, at, :] = both.astype(jnp.bfloat16)
                    return carry

                lax.fori_loop(0, rows // strip, add, 0)
                along(k).start()

    def after_4():
        for k in range(1, stack):
            along(k).wait_recv()

        def finish(i, carry):
            at, value = own_sum(0, i)
            for k in range(1, stack):
                value = value + far[k - 1, at, :].astype(jnp.float32)
            total[at, :] = value.astype(jnp.bfloat16)
            return carry

        lax.fori_loop(0, rows // strip, finish, 0)
        for s in range(1, groups):
            back(s).start()
        kept.start()

    tasks = {0: after_0, 1: after_1, 2: after_2, 3: after_3}

    for n, (u, s) in enumerate(jobs):
        w, c = units[u]
        load(n).wait()
        slot = n % SLOTS

        def convert(i, carry):
            at = pl.ds(pl.multiple_of(i * strip, strip), strip)
            value = stage[slot, at, :]
            if w < 2:
                gain = gain_ref[pl.ds(pl.multiple_of(c * height + i * strip, strip), strip), :]
                value = value * gain
            cast[u, s, at, :] = value.astype(jnp.bfloat16)
            return carry

        lax.fori_loop(0, height // strip, convert, 0)
        if n + SLOTS < len(jobs):
            load(n + SLOTS).start()
        if s == 0:
            pass_on(u, 0)
            if u >= 1:
                forward(u - 1)
            if u in tasks:
                tasks[u]()
        else:
            first(u, s).start()
    forward(len(units) - 1)
    pack(1)
    for k in range(stack):
        across(k).wait_send()
    after_4()
    for w in range(2):
        keep(w).wait()
        for c in range(chunks):
            arrived(w * chunks + c)
        fetch(w, expert).start()
    for w in range(2):
        fetch(w, expert).wait()
    hidden()
    keep(2).wait()
    for c in range(chunks):
        arrived(2 * chunks + c)
    fetch(2, expert).start()
    fetch(2, expert).wait()
    lower()
    done = pltpu.make_async_copy(partial, partial_out, last_sem.at[1])
    done.start()
    kept.wait()
    for s in range(1, groups):
        back(s).wait()
    for k in range(1, stack):
        along(k).wait_send()
    for u in range(len(units)):
        for s in range(groups):
            if s:
                first(u, s).wait_send()
            for b in range(blocks):
                goal, remote, local = second(u, s, b)

                @pl.when(goal != row)
                def _():
                    remote().wait_send()
    done.wait()


def serve(gain, gate, up, down, everything, spots, firsts, expert, collective):
    groups = lax.axis_size("tp")
    row_groups = lax.axis_size("fs")
    experts, rows, columns = gate.shape
    blocks = row_groups // groups
    width = columns // blocks
    model_width = rows * row_groups
    tokens = spots.shape[1]
    capacity = tokens // 2
    slots = groups * capacity
    chunks = 2
    units = 3 * chunks
    height = rows // chunks
    stack = row_groups // 2
    out = jax.ShapeDtypeStruct((experts // groups, model_width, width), jnp.bfloat16)
    hbm = pl.BlockSpec(memory_space=pl.ANY)
    vmem = pl.BlockSpec(memory_space=pltpu.VMEM)
    sent = 3 * rows * columns * 2 * groups
    weight = pltpu.VMEM((model_width, width), jnp.bfloat16)
    dma = lambda *shape: pltpu.SemaphoreType.DMA(shape)
    return pl.pallas_call(
        functools.partial(serve_kernel, groups, row_groups, expert, chunks),
        out_shape=(
            out, out, out,
            jax.ShapeDtypeStruct((groups, rows, capacity), jnp.bfloat16),
            jax.ShapeDtypeStruct((model_width, slots), jnp.bfloat16),
        ),
        in_specs=[vmem, hbm, hbm, hbm, hbm, vmem, hbm, hbm, hbm],
        out_specs=(hbm,) * 5,
        scratch_shapes=[
            pltpu.VMEM((SLOTS, height, columns), jnp.float32),
            pltpu.VMEM((units, groups, height, columns), jnp.bfloat16),
            pltpu.VMEM((units, groups - 1, height, columns), jnp.bfloat16),
            pltpu.VMEM((tokens, model_width), jnp.bfloat16),
            pltpu.VMEM((slots, model_width), jnp.bfloat16),
            weight, weight, weight,
            pltpu.VMEM((slots, width), jnp.bfloat16),
            pltpu.VMEM((model_width, slots), jnp.bfloat16),
            pltpu.VMEM((stack, rows, slots), jnp.bfloat16),
            pltpu.VMEM((stack - 1, rows, slots), jnp.bfloat16),
            pltpu.VMEM((stack - 1, rows, slots), jnp.bfloat16),
            pltpu.VMEM((rows, slots), jnp.bfloat16),
            dma(SLOTS), dma(units, groups - 1), dma(units, groups - 1),
            dma(units, row_groups), dma(units, row_groups),
            dma(row_groups), dma(3), dma(3),
            dma(stack), dma(stack), dma(stack - 1), dma(stack - 1),
            dma(groups - 1), dma(groups - 1), dma(2),
        ],
        compiler_params=pltpu.CompilerParams(
            collective_id=collective, has_side_effects=True, vmem_limit_bytes=62 * 1024 * 1024
        ),
        cost_estimate=pl.CostEstimate(
            flops=12 * slots * model_width * width, bytes_accessed=32 * sent, transcendentals=0
        ),
    )(gain, gate, up, down, everything, spots, *firsts)


def gather_sum_kernel(
    groups, row_groups, partial_ref, out_ref, own, pair, summed, far, total,
    load_sem, send_a, recv_a, send_b, recv_b, send_c, recv_c,
):
    me = lax.axis_index("tp")
    row = lax.axis_index("fs")
    side = lax.rem(row, 2)
    mate = row + 1 - 2 * side
    stack = row_groups // 2
    level = row // 2
    pieces, slots = total.shape
    capacity = slots // groups

    barrier = pltpu.get_barrier_semaphore()
    for step in range(1, groups):
        pl.semaphore_signal(
            barrier, inc=1, device_id={"tp": lax.rem(me + step, groups)}, device_id_type=MESH
        )
    for step in range(1, row_groups):
        pl.semaphore_signal(
            barrier, inc=1, device_id={"fs": lax.rem(row + step, row_groups)}, device_id_type=MESH
        )
    order = [stack // 2] + [k for k in range(1, stack) if k != stack // 2] + [0]

    def rows_of(k, which):
        goal = lax.rem(level + k, stack) * 2 + which
        return partial_ref.at[pl.ds(pl.multiple_of(goal * pieces, pieces), pieces)]

    def load(k):
        return pltpu.make_async_copy(rows_of(k, side), own.at[k], load_sem.at[k])

    def across(k):
        return pltpu.make_async_remote_copy(
            src_ref=rows_of(k, 1 - side),
            dst_ref=pair.at[k],
            send_sem=send_a.at[k],
            recv_sem=recv_a.at[k],
            device_id={"fs": mate},
            device_id_type=MESH,
        )

    def along(k):
        return pltpu.make_async_remote_copy(
            src_ref=summed.at[k],
            dst_ref=far.at[k],
            send_sem=send_b.at[k],
            recv_sem=recv_b.at[k],
            device_id={"fs": lax.rem(level + k, stack) * 2 + side},
            device_id_type=MESH,
        )

    def back(s):
        goal = lax.rem(me + s, groups)
        columns = pl.ds(pl.multiple_of(goal * capacity, capacity), capacity)
        return pltpu.make_async_remote_copy(
            src_ref=total.at[:, columns],
            dst_ref=out_ref.at[me],
            send_sem=send_c.at[s - 1],
            recv_sem=recv_c.at[s - 1],
            device_id={"tp": goal},
            device_id_type=MESH,
        )

    for k in order:
        load(k).start()
    pl.semaphore_wait(barrier, groups - 1 + row_groups - 1)
    for k in order:
        across(k).start()
    strip = 16
    for k in order:
        load(k).wait()
        across(k).wait_recv()

        def add(i, carry):
            at = pl.ds(pl.multiple_of(i * strip, strip), strip)
            both = own[k, at, :].astype(jnp.float32) + pair[k, at, :].astype(jnp.float32)
            summed[k, at, :] = both.astype(jnp.bfloat16)
            return carry

        if k:
            lax.fori_loop(0, pieces // strip, add, 0)
            along(k).start()
    for k in range(1, stack):
        along(k).wait_recv()

    def finish(i, carry):
        at = pl.ds(pl.multiple_of(i * strip, strip), strip)
        value = own[0, at, :].astype(jnp.float32) + pair[0, at, :].astype(jnp.float32)
        for k in range(1, stack):
            value = value + far[k, at, :].astype(jnp.float32)
        total[at, :] = value.astype(jnp.bfloat16)
        return carry

    lax.fori_loop(0, pieces // strip, finish, 0)
    for s in range(1, groups):
        back(s).start()
    columns = pl.ds(pl.multiple_of(me * capacity, capacity), capacity)
    kept = pltpu.make_async_copy(total.at[:, columns], out_ref.at[me], load_sem.at[0])
    kept.start()
    kept.wait()
    for s in range(1, groups):
        back(s).wait()
    for k in range(stack):
        across(k).wait_send()
        if k:
            along(k).wait_send()


def gather_sum(partial, collective):
    groups = lax.axis_size("tp")
    row_groups = lax.axis_size("fs")
    model_width, slots = partial.shape
    pieces = model_width // row_groups
    stack = row_groups // 2
    capacity = slots // groups
    block = pltpu.VMEM((stack, pieces, slots), jnp.bfloat16)
    sent = model_width * slots * 2
    return pl.pallas_call(
        functools.partial(gather_sum_kernel, groups, row_groups),
        out_shape=jax.ShapeDtypeStruct((groups, pieces, capacity), jnp.bfloat16),
        in_specs=[pl.BlockSpec(memory_space=pl.ANY)],
        out_specs=pl.BlockSpec(memory_space=pl.ANY),
        scratch_shapes=[
            block, block, block, block,
            pltpu.VMEM((pieces, slots), jnp.bfloat16),
            pltpu.SemaphoreType.DMA((stack,)),
            pltpu.SemaphoreType.DMA((stack,)),
            pltpu.SemaphoreType.DMA((stack,)),
            pltpu.SemaphoreType.DMA((stack,)),
            pltpu.SemaphoreType.DMA((stack,)),
            pltpu.SemaphoreType.DMA((groups - 1,)),
            pltpu.SemaphoreType.DMA((groups - 1,)),
        ],
        compiler_params=pltpu.CompilerParams(
            collective_id=collective, has_side_effects=True, vmem_limit_bytes=20 * 1024 * 1024
        ),
        cost_estimate=pl.CostEstimate(
            flops=sent, bytes_accessed=32 * sent, transcendentals=0
        ),
    )(partial)


def fused_device(
    hidden_states, norm_gain, gate_master, up_master, down_master, expert_ids, route_logits
):
    groups = lax.axis_size("tp")
    row_groups = lax.axis_size("fs")
    experts = gate_master.shape[0]
    local_count = experts // groups
    tokens, pieces = hidden_states.shape
    model_width = pieces * row_groups
    capacity = tokens // 2
    me = lax.axis_index("tp")
    gain = norm_gain[:, None]
    id_rows = expert_ids.size // pieces
    sheet = expert_ids.astype(jnp.bfloat16).reshape(id_rows, pieces)
    sheet = jnp.pad(sheet, ((0, -id_rows % 16), (0, 0)))
    everything = lax.all_gather(jnp.concatenate([hidden_states, sheet]), ("fs", "tp"), axis=0)
    everything = everything.reshape(row_groups, groups, -1, pieces)
    all_ids = everything[0, :, tokens : tokens + id_rows].astype(jnp.int32)
    all_ids = all_ids.reshape(groups, tokens, 2)
    earlier = (jnp.arange(tokens)[:, None] > jnp.arange(tokens)[None, :]).astype(jnp.bfloat16)
    weights = jax.nn.softmax(route_logits, axis=1)
    named = expert_ids[:, :, None] == jnp.arange(experts, dtype=jnp.int32)[None, None, :]
    chosen = jnp.any(named, axis=1).astype(jnp.bfloat16)
    before = jnp.dot(earlier, chosen, preferred_element_type=jnp.float32)
    position = jnp.sum(jnp.where(named, before[:, None, :], 0.0), axis=2).astype(jnp.int32)
    slot_ids = (expert_ids * capacity + position).reshape(-1)

    mine = jnp.any(
        all_ids[None] == (me * local_count + jnp.arange(local_count))[:, None, None, None], axis=3
    )
    spots = jnp.einsum(
        "ts,jgs->jgt", earlier, mine.astype(jnp.bfloat16), preferred_element_type=jnp.float32
    ).astype(jnp.int32)
    spots = jnp.where(mine, spots, -1).reshape(local_count * groups, tokens)
    firsts = exchange(gain, gate_master, up_master, down_master, hidden_states, 0, 1)
    gate, up, down, early, partial = serve(
        gain, gate_master, up_master, down_master, everything, spots, firsts, 1, 2
    )
    last = gather_sum(partial, 3)
    ordered = jnp.stack([early, last], axis=1)
    flat_out = jnp.moveaxis(ordered, 2, 0).reshape(pieces, experts * capacity)
    picked = flat_out.at[:, slot_ids].get(mode="promise_in_bounds")
    picked = picked.reshape(pieces, tokens, 2).astype(jnp.float32)
    combined = jnp.sum(picked * weights[None, :, :], axis=2)
    return gate, up, down, jnp.transpose(combined).astype(jnp.bfloat16)


def arrange(weights, groups, row_groups):
    experts, rows, columns = weights.shape
    blocks = row_groups // groups
    split = weights.reshape(experts // groups, groups, rows, blocks, columns // blocks)
    split = split.reshape(groups, experts // groups, rows, blocks, columns // blocks)
    return jnp.transpose(split, (0, 3, 1, 2, 4))


def regroup(moved, row_groups):
    return moved.reshape((row_groups,) + moved.shape[2:])


def settle(arrived):
    return arrived.reshape(arrived.shape[1], arrived.shape[2], arrived.shape[3])


def per_device(
    hidden_states, norm_gain, gate_master, up_master, down_master, expert_ids, route_logits
):
    groups = lax.axis_size("tp")
    row_groups = lax.axis_size("fs")
    whole_tiles = gate_master.shape[2] // (row_groups // groups) % 128 == 0
    if whole_tiles and gate_master.shape[0] == 2 * groups and row_groups % 4 == 0 and expert_ids.size % hidden_states.shape[1] == 0:
        return fused_device(
            hidden_states, norm_gain, gate_master, up_master, down_master, expert_ids, route_logits
        )
    experts = gate_master.shape[0]
    local_count = experts // groups
    tokens = hidden_states.shape[0]
    pieces = hidden_states.shape[1]
    model_width = pieces * row_groups
    capacity = tokens // 2
    scaled = norm_gain[None, :, None]
    gate_cast = arrange((scaled * gate_master).astype(jnp.bfloat16), groups, row_groups)
    up_cast = arrange((scaled * up_master).astype(jnp.bfloat16), groups, row_groups)
    down_cast = arrange(down_master.astype(jnp.bfloat16), groups, row_groups)
    sectioned = (
        lax.all_to_all(gate_cast, "tp", split_axis=0, concat_axis=0, tiled=True),
        lax.all_to_all(up_cast, "tp", split_axis=0, concat_axis=0, tiled=True),
        lax.all_to_all(down_cast, "tp", split_axis=0, concat_axis=0, tiled=True),
    )
    landed = (
        lax.all_to_all(
            regroup(sectioned[0], row_groups), "fs", split_axis=0, concat_axis=2, tiled=True
        ),
        lax.all_to_all(
            regroup(sectioned[1], row_groups), "fs", split_axis=0, concat_axis=2, tiled=True
        ),
        lax.all_to_all(
            regroup(sectioned[2], row_groups), "fs", split_axis=0, concat_axis=2, tiled=True
        ),
    )
    gate_serve, up_serve, down_serve = (settle(landed[0]), settle(landed[1]), settle(landed[2]))
    values = hidden_states.astype(jnp.float32)
    squares = lax.psum(jnp.sum(values * values, axis=1), "fs")
    normed = (values * lax.rsqrt(squares / model_width + EPSILON)[:, None]).astype(jnp.bfloat16)
    weights = jax.nn.softmax(route_logits, axis=1)
    chosen = (expert_ids[:, :, None] == jnp.arange(experts, dtype=jnp.int32)[None, None, :]).astype(
        jnp.int32
    )
    chosen = chosen.reshape(tokens * 2, experts)
    before = jnp.cumsum(chosen, axis=0) - chosen
    position = jnp.sum(before * chosen, axis=1)
    slot_ids = expert_ids.reshape(-1) * capacity + position
    slot_table = (
        slot_ids[None, :] == jnp.arange(experts * capacity, dtype=jnp.int32)[:, None]
    ).astype(jnp.bfloat16)
    dispatch = jnp.sum(slot_table.reshape(experts * capacity, tokens, 2), axis=2)
    whole_rows = lax.all_gather(normed, "fs", axis=1, tiled=True)
    packed = jnp.dot(dispatch, whole_rows, preferred_element_type=jnp.float32).astype(jnp.bfloat16)
    arrived = lax.all_to_all(
        packed.reshape(groups, local_count * capacity, model_width),
        "tp",
        split_axis=0,
        concat_axis=0,
        tiled=True,
    )
    arranged = arrived.reshape(groups, local_count, capacity, model_width)
    activations = []
    for expert_index in range(local_count):
        expert_rows = arranged[:, expert_index].reshape(groups * capacity, model_width)
        gate_pre = jnp.dot(
            expert_rows, gate_serve[expert_index], preferred_element_type=jnp.float32
        )
        up_pre = jnp.dot(expert_rows, up_serve[expert_index], preferred_element_type=jnp.float32)
        activations.append((jax.nn.silu(gate_pre) * up_pre).astype(jnp.bfloat16))
    stacked = jnp.stack(activations)
    summed = lax.psum_scatter(
        jnp.einsum("jdh,jsh->djs", down_serve, stacked, preferred_element_type=jnp.float32).astype(
            jnp.bfloat16
        ),
        "fs",
        scatter_dimension=0,
        tiled=True,
    )
    results = summed.reshape(pieces, local_count, groups, capacity)
    returned = lax.all_to_all(results, "tp", split_axis=2, concat_axis=1, tiled=True)
    flat_out = returned.reshape(pieces, experts * capacity)
    picked = jnp.take(flat_out, slot_ids, axis=1).reshape(pieces, tokens, 2).astype(jnp.float32)
    combined = jnp.sum(picked * weights[None, :, :], axis=2)
    return (gate_serve, up_serve, down_serve, jnp.transpose(combined).astype(jnp.bfloat16))


def solution(mesh):
    in_specs = (
        P("tp", "fs"),
        P("fs"),
        P(None, "fs", "tp"),
        P(None, "fs", "tp"),
        P(None, "fs", "tp"),
        P("tp", None),
        P("tp", None),
    )
    out_specs = (P("tp", None, "fs"), P("tp", None, "fs"), P("tp", None, "fs"), P("tp", "fs"))
    return jax.shard_map(
        per_device, mesh=mesh, in_specs=in_specs, out_specs=out_specs, check_vma=False
    )
```

profile of v0, /device:TPU:0, one launch (start us, length us, event | category | flops | bytes accessed | tf_op | source)
XLA Modules:
  0.0 745.0 jit_solution(8516543213319447670)
XLA Ops:
  7.2 0.0 all-gather.3.cloned.1.call-start
  7.2 0.7 fusion.6
  7.9 0.2 fusion.1
  8.1 0.7 select_reduce_fusion
  8.9 0.8 convert_add_fusion
  9.6 0.2 copy.24
  9.8 0.2 reshape.70
  10.0 1.7 fusion.5
  11.7 0.0 all-gather.3.cloned.1.call-update
  11.7 0.8 copy.28.gain_ref
  12.5 0.0 copy-start.1
  12.6 0.9 copy-done.1
  13.5 0.0 copy-start.2
  13.5 0.0 copy-start.5
  13.5 264.0 %shard_map.102 = (bf16[2048,896]{1,0:T(8,128)(2,1)S(1)}, bf16[2048,896]{1,0:T(8,128)(2,1)S(1)}, bf16[2048,896]{1,0:T(8,128)(2,1)}) custom-call(f32[256,1]{1,0:T(8,128)S(1)} %copy.28.gain_ref, f32[8,256,1792]{2,1,0:T(8,128)} %gate_ref.3, f32[8,256,1792]{2,1,0:T(8,128)} %up_ref.3, f32[8,256,1792]{2,1,0:T(8,128)} %down_ref.3, bf16[512,256]{1,0:T(8,128)(2,1)S(1)} %copy-done.1), custom_call_target="tpu_custom_call" | custom-call | flops 458752 | bytes 352321536 | tf_op jit(solution)/shard_map/pallas_call | solution.py:157
  277.5 0.0 copy-done.2
  277.5 0.0 copy-start.3
  277.5 1.8 copy-done.3
  279.3 0.0 copy-start.4
  279.3 1.8 copy-done.4
  281.2 0.1 copy.30
  281.3 0.2 reshape.74
  281.5 0.0 copy-done.5
  281.6 0.1 copy.31
  281.8 0.0 all-gather.3.cloned.1.call-done
  281.8 0.7 slice_convert_fusion
  282.5 0.2 copy.25
  282.8 0.2 copy.26
  283.0 0.1 compare_reduce_fusion
  283.1 0.3 fusion
  283.3 0.6 reshape.72.spot_ref
  284.0 314.9 %shard_map.103 = (bf16[2,2048,896]{2,1,0:T(8,128)(2,1)}, bf16[2,2048,896]{2,1,0:T(8,128)(2,1)}, bf16[2,2048,896]{2,1,0:T(8,128)(2,1)}, bf16[4,256,256]{2,1,0:T(8,128)(2,1)}, bf16[2048,1024]{1,0:T(8,128)(2,1)}) custom-call(f32[256,1]{1,0:T(8,128)} %copy-done.2, f32[8,256,1792]{2,1,0:T(8,128)} %gate_ref.3, f32[8,256,1792]{2,1,0:T(8,128)} %up_ref.3, ...), custom_call_target="tpu_custom_call" | custom-call | flops 22548578304 | bytes 352321536 | tf_op jit(solution)/shard_map/pallas_call | solution.py:521
  598.9 0.0 copy-start
  598.9 2.2 copy-done
  601.1 110.2 %shard_map.104 = bf16[4,256,256]{2,1,0:T(8,128)(2,1)S(1)} custom-call(bf16[2048,1024]{1,0:T(8,128)(2,1)S(1)} %copy-done), custom_call_target="tpu_custom_call" | custom-call | flops 4194304 | bytes 134217728 | tf_op jit(solution)/shard_map/pallas_call | solution.py:675
  711.3 1.1 maximum_bitcast_fusion
  712.5 0.5 copy.29
  713.0 3.9 gather_fusion
  716.9 0.1 convert_bitcast_fusion
  717.0 0.6 reshape.76
  717.6 3.8 multiply_reduce_fusion
  721.4 0.0 slice-start
  721.4 6.9 copy.35
  728.3 0.0 slice-start.1
  728.3 6.9 copy.36
  735.1 0.0 slice-done
  735.1 0.0 slice-done.1
  735.1 3.0 copy.37
  (7 shorter events, 0.1 us)
Async XLA Ops:
  7.2 274.7 %all-gather.3.cloned.1.call-start = ((), (), s32[]{:S(2)}) async-start(), calls=%async_computation | async-start | bytes 8921088 | tf_op jit(solution)/shard_map/all_gather | solution.py:715
  12.5 1.0 copy-start.1
  13.5 264.0 %copy-start.2 = (f32[256,1]{1,0:T(8,128)}, f32[256,1]{1,0:T(8,128)S(1)}, u32[]{:S(2)}) copy-start(f32[256,1]{1,0:T(8,128)S(1)} %copy.28.gain_ref) | copy-start | bytes 3076
  13.5 268.0 %copy-start.5 = (f32[512,2]{0,1:T(2,128)S(1)}, f32[512,2]{0,1:T(2,128)}, u32[]{:S(2)}) copy-start(f32[512,2]{0,1:T(2,128)} %param.13) | copy-start | bytes 12292
  277.5 1.8 copy-start.3
  279.3 1.8 copy-start.4
  598.9 2.2 copy-start
  721.4 13.7 %slice-start = ((s8[7340032]{0:T(1024)(128)(4,1)}), s8[4194304]{0:T(1024)(128)(4,1)S(1)}, s32[]{:S(2)}) async-start(s8[7340032]{0:T(1024)(128)(4,1)} %bitcast.23), calls=%async_computation.1 | async-start | bytes 8388608
  728.3 6.9 slice-start.1
Sparse Core Ops, SparseCore 0:
  11.8 174.8 all-gather.2
where the time goes:
time: 746 us; the launch traced here: 745 us
  Pallas kernels  689 us (92%)
  local copies, waits for them, and re-layouts  31.4 us (4%)
  between operations  14.2 us (2%)
  other arithmetic  9.76 us (1%)
    pallas_call x1, Pallas kernels, serve(): pl.pallas_call(functools.partial(serve_kernel, groups, row_groups, expert...  315 us
    pallas_call x1, Pallas kernels, exchange(): pl.pallas_call(functools.partial(exchange_kernel, groups, row_groups, exp...  264 us
    pallas_call x1, Pallas kernels, gather_sum(): pl.pallas_call(functools.partial(gather_sum_kernel, groups, row_groups),...  110 us
    unnamed x19, local copies, waits for them, and re-layouts  23.6 us
  transfers between devices with their start and end apart: 1, of which 0 were waited for; matrix products, arithmetic and copies ran while one was open for 0% of the time, Pallas kernels for 35%

commit v1 on v0

--- a/solution.py
+++ b/solution.py
@@ -13,9 +13,10 @@
 
 
 def exchange_kernel(
-    groups, row_groups, expert, chunks, gain_ref, gate_ref, up_ref, down_ref, dep_ref,
-    gate_out, up_out, down_out, stage, cast, landed, load_sem,
-    send_a, recv_a, send_b, recv_b,
+    groups, row_groups, expert, chunks, gain_ref, gate_ref, up_ref, down_ref, own_ref, spot_ref,
+    gate_out, up_out, down_out, all_out, spot_out, stage, cast, landed, load_sem,
+    send_a, recv_a, send_b, recv_b, send_z, recv_z, send_y, recv_y, send_t, recv_t,
+    send_s, recv_s, own_sem,
 ):
     me = lax.axis_index("tp")
     row = lax.axis_index("fs")
@@ -101,6 +102,83 @@
             first(u, s).wait_recv()
             pass_on(u, s)
 
+    side = lax.rem(row, 2)
+    mate = row + 1 - 2 * side
+    stack = row_groups // 2
+    level = row // 2
+
+    def block(k, y):
+        which = side if y == 0 else 1 - side
+        return lax.rem(level + stack - k, stack) * 2 + which
+
+    def up_z(k):
+        return pltpu.make_async_remote_copy(
+            src_ref=own_ref,
+            dst_ref=all_out.at[row, me],
+            send_sem=send_z.at[k - 1],
+            recv_sem=recv_z.at[k - 1],
+            device_id={"fs": lax.rem(level + k, stack) * 2 + side},
+            device_id_type=MESH,
+        )
+
+    def over_y(k):
+        place = all_out.at[block(k, 0), me]
+        return pltpu.make_async_remote_copy(
+            src_ref=own_ref if k == 0 else place,
+            dst_ref=place,
+            send_sem=send_y.at[k],
+            recv_sem=recv_y.at[k],
+            device_id={"fs": mate},
+            device_id_type=MESH,
+        )
+
+    def over_tp(k, y, s):
+        place = all_out.at[block(k, y), me]
+        return pltpu.make_async_remote_copy(
+            src_ref=own_ref if k == 0 and y == 0 else place,
+            dst_ref=place,
+            send_sem=send_t.at[y * stack + k, s - 1],
+            recv_sem=recv_t.at[y * stack + k, s - 1],
+            device_id={"tp": lax.rem(me + s, groups)},
+            device_id_type=MESH,
+        )
+
+    def spots_to(s):
+        goal = lax.rem(me + s, groups)
+        return pltpu.make_async_remote_copy(
+            src_ref=spot_ref.at[goal],
+            dst_ref=spot_out.at[me],
+            send_sem=send_s.at[s - 1],
+            recv_sem=recv_s.at[s - 1],
+            device_id={"tp": goal},
+            device_id_type=MESH,
+        )
+
+    own_kept = pltpu.make_async_copy(own_ref, all_out.at[row, me], own_sem.at[0])
+    spot_kept = pltpu.make_async_copy(spot_ref.at[me], spot_out.at[me], own_sem.at[1])
+    own_kept.start()
+    spot_kept.start()
+    for k in range(1, stack):
+        up_z(k).start()
+    over_y(0).start()
+    for s in range(1, groups):
+        spots_to(s).start()
+
+    def near_blocks():
+        for k in range(stack):
+            if k:
+                up_z(k).wait_recv()
+                over_y(k).start()
+            for s in range(1, groups):
+                over_tp(k, 0, s).start()
+
+    def far_blocks():
+        for k in range(stack):
+            over_y(k).wait_recv()
+            for s in range(1, groups):
+                over_tp(k, 1, s).start()
+
+    tasks = {1: near_blocks, 3: far_blocks}
     strip = 16
     for n, (u, s) in enumerate(jobs):
         w, c = units[u]
@@ -123,9 +201,22 @@
             pass_on(u, 0)
             if u >= 1:
                 forward(u - 1)
+            if u in tasks:
+                tasks[u]()
         else:
             first(u, s).start()
     forward(len(units) - 1)
+    own_kept.wait()
+    spot_kept.wait()
+    for k in range(stack):
+        if k:
+            up_z(k).wait_send()
+        over_y(k).wait_send()
+        for s in range(1, groups):
+            for y in range(2):
+                over_tp(k, y, s).wait()
+    for s in range(1, groups):
+        spots_to(s).wait()
     for u in range(len(units)):
         for s in range(groups):
             if s:
@@ -142,7 +233,7 @@
             ).wait()
 
 
-def exchange(gain, gate, up, down, dep, expert, collective):
+def exchange(gain, gate, up, down, hidden, spots, expert, collective):
     groups = lax.axis_size("tp")
     row_groups = lax.axis_size("fs")
     experts, rows, columns = gate.shape
@@ -153,21 +244,28 @@
     height = rows // chunks
     out = jax.ShapeDtypeStruct((rows * row_groups, width), jnp.bfloat16)
     hbm = pl.BlockSpec(memory_space=pl.ANY)
+    stack = row_groups // 2
+    vmem = pl.BlockSpec(memory_space=pltpu.VMEM)
     sent = 3 * rows * columns * 2 * groups
+    dma = lambda *shape: pltpu.SemaphoreType.DMA(shape)
     return pl.pallas_call(
         functools.partial(exchange_kernel, groups, row_groups, expert, chunks),
-        out_shape=(out, out, out),
-        in_specs=[pl.BlockSpec(memory_space=pltpu.VMEM), hbm, hbm, hbm, hbm],
-        out_specs=(hbm, hbm, hbm),
+        out_shape=(
+            out, out, out,
+            jax.ShapeDtypeStruct((row_groups, groups) + hidden.shape, hidden.dtype),
+            jax.ShapeDtypeStruct(spots.shape, spots.dtype),
+        ),
+        in_specs=[vmem, hbm, hbm, hbm, vmem, vmem],
+        out_specs=(hbm,) * 5,
         scratch_shapes=[
             pltpu.VMEM((SLOTS, height, columns), jnp.float32),
             pltpu.VMEM((units, groups, height, columns), jnp.bfloat16),
             pltpu.VMEM((units, groups - 1, height, columns), jnp.bfloat16),
-            pltpu.SemaphoreType.DMA((SLOTS,)),
-            pltpu.SemaphoreType.DMA((units, groups - 1)),
-            pltpu.SemaphoreType.DMA((units, groups - 1)),
-            pltpu.SemaphoreType.DMA((units, row_groups)),
-            pltpu.SemaphoreType.DMA((units, row_groups)),
+            dma(SLOTS), dma(units, groups - 1), dma(units, groups - 1),
+            dma(units, row_groups), dma(units, row_groups),
+            dma(stack - 1), dma(stack - 1), dma(stack), dma(stack),
+            dma(2 * stack, groups - 1), dma(2 * stack, groups - 1),
+            dma(groups - 1), dma(groups - 1), dma(2),
         ],
         compiler_params=pltpu.CompilerParams(
             collective_id=collective, has_side_effects=True, vmem_limit_bytes=44 * 1024 * 1024
@@ -175,16 +273,17 @@
         cost_estimate=pl.CostEstimate(
             flops=rows * columns, bytes_accessed=32 * sent, transcendentals=0
         ),
-    )(gain, gate, up, down, dep)
+    )(gain, gate, up, down, hidden, spots)
 
 
 def serve_kernel(
     groups, row_groups, expert, chunks, gain_ref, gate_ref, up_ref, down_ref, all_ref, spot_ref,
     gate_first, up_first, down_first,
-    gate_out, up_out, down_out, early_out, partial_out,
-    stage, cast, landed, raw, rows_in, gate_w, up_w, down_w, act, partial, pair, summed, far, total,
+    gate_out, up_out, down_out, back_out,
+    stage, cast, landed, raw, rows_in, gate_w, up_w, down_w, act, partial,
+    pair, to_near, near, to_far, far, total,
     load_sem, send_a, recv_a, send_b, recv_b, raw_sem, weight_sem, keep_sem,
-    send_c, recv_c, send_d, recv_d, send_e, recv_e, last_sem,
+    send_c, recv_c, send_d, recv_d, send_f, recv_f, send_e, recv_e, last_sem,
 ):
     me = lax.axis_index("tp")
     row = lax.axis_index("fs")
@@ -279,17 +378,16 @@
             first(u, s).wait_recv()
             pass_on(u, s)
 
-    def arrived(u):
-        for source in range(row_groups):
-            pltpu.make_async_copy(
-                cast.at[u, 0, :, pl.ds(0, width)], place(u, source), recv_b.at[u, source]
-            ).wait()
+    def arrived(u, source):
+        pltpu.make_async_copy(
+            cast.at[u, 0, :, pl.ds(0, width)], place(u, source), recv_b.at[u, source]
+        ).wait()
 
     def pack(j):
         def one(g, carry):
             copies = [
                 pltpu.make_async_copy(
-                    all_ref.at[f, g, pl.ds(0, tokens)],
+                    all_ref.at[f, g],
                     raw.at[:, pl.ds(f * (model_width // row_groups), model_width // row_groups)],
                     raw_sem.at[f],
                 )
@@ -299,8 +397,8 @@
                 copy.start()
             for copy in copies:
                 copy.wait()
-            spot = spot_ref[pl.ds(j * groups + g, 1), :]
-            slot = lax.broadcasted_iota(jnp.int32, (capacity, tokens), 0)
+            spot = spot_ref[g, pl.ds(j, 1), :]
+            slot = lax.broadcasted_iota(jnp.int32, (capacity, tokens), 0).astype(jnp.float32)
             table = jnp.where(slot == spot, 1.0, 0.0).astype(jnp.bfloat16)
             packed = jnp.dot(table, raw[...], preferred_element_type=jnp.float32)
             mean = jnp.mean(packed * packed, axis=1, keepdims=True)
@@ -321,15 +419,11 @@
 
         lax.fori_loop(0, groups, one, 0)
 
-    def lower():
-        def one(r, carry):
-            at = pl.ds(pl.multiple_of(r * rows, rows), rows)
-            partial[at, :] = lax.dot_general(
-                down_w[at, :], act[...], (((1,), (1,)), ((), ())), preferred_element_type=jnp.float32
-            ).astype(jnp.bfloat16)
-            return carry
-
-        lax.fori_loop(0, row_groups, one, 0)
+    def lower(r):
+        at = pl.ds(pl.multiple_of(r * rows, rows), rows)
+        partial[at, :] = lax.dot_general(
+            down_w[at, :], act[...], (((1,), (1,)), ((), ())), preferred_element_type=jnp.float32
+        ).astype(jnp.bfloat16)
 
     def fetch(w, j):
         source = firsts[w] if j == 0 else outs[w].at[j]
@@ -338,52 +432,91 @@
     def keep(w):
         return pltpu.make_async_copy(held_w[w], outs[w].at[0], keep_sem.at[w])
 
-    levels = [stack // 2] + [k for k in range(1, stack) if k != stack // 2] + [0]
-
-    def rows_of(k, which):
-        return (lax.rem(level + k, stack) * 2 + which) * rows
-
-    def across(k):
-        return pltpu.make_async_remote_copy(
-            src_ref=partial.at[pl.ds(pl.multiple_of(rows_of(k, 1 - side), rows), rows)],
-            dst_ref=pair.at[k],
-            send_sem=send_c.at[k],
-            recv_sem=recv_c.at[k],
+    def level_at(d):
+        return lax.rem(level // 2 + d // 2, 2) * 2 + lax.rem(level + d, 2)
+
+    def across(j, d):
+        goal = level_at(d) * 2 + 1 - side
+        return pltpu.make_async_remote_copy(
+            src_ref=partial.at[pl.ds(pl.multiple_of(goal * rows, rows), rows)],
+            dst_ref=pair.at[j, d],
+            send_sem=send_c.at[j, d],
+            recv_sem=recv_c.at[j, d],
             device_id={"fs": mate},
             device_id_type=MESH,
         )
 
-    def along(k):
-        return pltpu.make_async_remote_copy(
-            src_ref=summed.at[k - 1],
-            dst_ref=far.at[k - 1],
-            send_sem=send_d.at[k - 1],
-            recv_sem=recv_d.at[k - 1],
-            device_id={"fs": lax.rem(level + k, stack) * 2 + side},
-            device_id_type=MESH,
-        )
-
-    def back(s):
+    def along_near(j, d):
+        return pltpu.make_async_remote_copy(
+            src_ref=to_near.at[j, d - 1],
+            dst_ref=near.at[j, d - 1],
+            send_sem=send_d.at[j, d - 1],
+            recv_sem=recv_d.at[j, d - 1],
+            device_id={"fs": level_at(1) * 2 + side},
+            device_id_type=MESH,
+        )
+
+    def along_far(j):
+        return pltpu.make_async_remote_copy(
+            src_ref=to_far.at[j],
+            dst_ref=far.at[j],
+            send_sem=send_f.at[j],
+            recv_sem=recv_f.at[j],
+            device_id={"fs": level_at(3) * 2 + side},
+            device_id_type=MESH,
+        )
+
+    def back(j, s):
         goal = lax.rem(me + s, groups)
         return pltpu.make_async_remote_copy(
-            src_ref=total.at[:, pl.ds(pl.multiple_of(goal * capacity, capacity), capacity)],
-            dst_ref=early_out.at[me],
-            send_sem=send_e.at[s - 1],
-            recv_sem=recv_e.at[s - 1],
+            src_ref=total.at[j, :, pl.ds(pl.multiple_of(goal * capacity, capacity), capacity)],
+            dst_ref=back_out.at[me, j],
+            send_sem=send_e.at[j, s - 1],
+            recv_sem=recv_e.at[j, s - 1],
             device_id={"tp": goal},
             device_id_type=MESH,
         )
 
-    kept = pltpu.make_async_copy(
-        total.at[:, pl.ds(pl.multiple_of(me * capacity, capacity), capacity)],
-        early_out.at[me],
-        last_sem.at[0],
-    )
-
-    def own_sum(k, i):
-        at = pl.ds(pl.multiple_of(i * strip, strip), strip)
-        mine = pl.ds(pl.multiple_of(rows_of(k, side) + i * strip, strip), strip)
-        return at, partial[mine, :].astype(jnp.float32) + pair[k, at, :].astype(jnp.float32)
+    def kept(j):
+        return pltpu.make_async_copy(
+            total.at[j, :, pl.ds(pl.multiple_of(me * capacity, capacity), capacity)],
+            back_out.at[me, j],
+            last_sem.at[j],
+        )
+
+    def sum_into(j, d, target, others):
+        base = (level_at(d) * 2 + side) * rows
+
+        def add(i, carry):
+            at = pl.ds(pl.multiple_of(i * strip, strip), strip)
+            mine = pl.ds(pl.multiple_of(base + i * strip, strip), strip)
+            value = partial[mine, :].astype(jnp.float32) + pair[j, d, at, :].astype(jnp.float32)
+            for other in others:
+                value = value + other[at, :].astype(jnp.float32)
+            target[at, :] = value.astype(jnp.bfloat16)
+            return carry
+
+        lax.fori_loop(0, rows // strip, add, 0)
+
+    def to_level(j, d):
+        across(j, d).wait_recv()
+        sum_into(j, d, to_near.at[j, d - 1], ())
+        along_near(j, d).start()
+
+    def cross_over(j):
+        across(j, 3).wait_recv()
+        along_near(j, 2).wait_recv()
+        sum_into(j, 3, to_far.at[j], (near.at[j, 1],))
+        along_far(j).start()
+
+    def settle_sum(j):
+        across(j, 0).wait_recv()
+        along_near(j, 1).wait_recv()
+        along_far(j).wait_recv()
+        sum_into(j, 0, total.at[j], (near.at[j, 0], far.at[j]))
+        for s in range(1, groups):
+            back(j, s).start()
+        kept(j).start()
 
     def after_0():
         for w in range(len(masters)):
@@ -399,40 +532,23 @@
     def after_2():
         fetch(2, 0).wait()
         keep(2).start()
-        lower()
-        for k in levels:
-            across(k).start()
+
+        def one(r, carry):
+            lower(r)
+            return carry
+
+        lax.fori_loop(0, row_groups, one, 0)
+        for d in range(stack):
+            across(0, d).start()
 
     def after_3():
-        for k in levels:
-            across(k).wait_recv()
-            if k:
-
-                def add(i, carry):
-                    at, both = own_sum(k, i)
-                    summed[k - 1, at, :] = both.astype(jnp.bfloat16)
-                    return carry
-
-                lax.fori_loop(0, rows // strip, add, 0)
-                along(k).start()
+        to_level(0, 1)
+        to_level(0, 2)
 
     def after_4():
-        for k in range(1, stack):
-            along(k).wait_recv()
-
-        def finish(i, carry):
-            at, value = own_sum(0, i)
-            for k in range(1, stack):
-                value = value + far[k - 1, at, :].astype(jnp.float32)
-            total[at, :] = value.astype(jnp.bfloat16)
-            return carry
-
-        lax.fori_loop(0, rows // strip, finish, 0)
-        for s in range(1, groups):
-            back(s).start()
-        kept.start()
-
-    tasks = {0: after_0, 1: after_1, 2: after_2, 3: after_3}
+        cross_over(0)
+
+    tasks = {0: after_0, 1: after_1, 2: after_2, 3: after_3, 4: after_4}
 
     for n, (u, s) in enumerate(jobs):
         w, c = units[u]
@@ -461,30 +577,54 @@
             first(u, s).start()
     forward(len(units) - 1)
     pack(1)
-    for k in range(stack):
-        across(k).wait_send()
-    after_4()
+    settle_sum(0)
+    for d in range(stack):
+        across(0, d).wait_send()
     for w in range(2):
         keep(w).wait()
         for c in range(chunks):
-            arrived(w * chunks + c)
+            for source in range(row_groups):
+                arrived(w * chunks + c, source)
         fetch(w, expert).start()
     for w in range(2):
         fetch(w, expert).wait()
     hidden()
     keep(2).wait()
-    for c in range(chunks):
-        arrived(2 * chunks + c)
-    fetch(2, expert).start()
-    fetch(2, expert).wait()
-    lower()
-    done = pltpu.make_async_copy(partial, partial_out, last_sem.at[1])
-    done.start()
-    kept.wait()
-    for s in range(1, groups):
-        back(s).wait()
-    for k in range(1, stack):
-        along(k).wait_send()
+
+    def piece(d, i):
+        r = level_at(d) * 2 + lax.rem(side + 1 + i, 2)
+        at = pl.ds(pl.multiple_of(r * rows, rows), rows)
+        copy = pltpu.make_async_copy(outs[2].at[expert, at], down_w.at[at], raw_sem.at[i])
+        return r, copy
+
+    for d in range(stack):
+        for i in range(2):
+            r, copy = piece(d, i)
+            for c in range(chunks):
+                arrived(2 * chunks + c, r)
+            copy.start()
+        for i in range(2):
+            piece(d, i)[1].wait()
+
+        def one(i, carry):
+            lower(level_at(d) * 2 + lax.rem(side + 1 + i, 2))
+            return carry
+
+        lax.fori_loop(0, 2, one, 0)
+        across(1, d).start()
+        if d >= 2:
+            to_level(1, d - 1)
+    cross_over(1)
+    settle_sum(1)
+    for d in range(stack):
+        across(1, d).wait_send()
+    for j in range(2):
+        for d in (1, 2):
+            along_near(j, d).wait_send()
+        along_far(j).wait_send()
+        kept(j).wait()
+        for s in range(1, groups):
+            back(j, s).wait()
     for u in range(len(units)):
         for s in range(groups):
             if s:
@@ -495,7 +635,6 @@
                 @pl.when(goal != row)
                 def _():
                     remote().wait_send()
-    done.wait()
 
 
 def serve(gain, gate, up, down, everything, spots, firsts, expert, collective):
@@ -505,7 +644,7 @@
     blocks = row_groups // groups
     width = columns // blocks
     model_width = rows * row_groups
-    tokens = spots.shape[1]
+    tokens = spots.shape[2]
     capacity = tokens // 2
     slots = groups * capacity
     chunks = 2
@@ -522,11 +661,10 @@
         functools.partial(serve_kernel, groups, row_groups, expert, chunks),
         out_shape=(
             out, out, out,
-            jax.ShapeDtypeStruct((groups, rows, capacity), jnp.bfloat16),
-            jax.ShapeDtypeStruct((model_width, slots), jnp.bfloat16),
+            jax.ShapeDtypeStruct((groups, 2, rows, capacity), jnp.bfloat16),
         ),
         in_specs=[vmem, hbm, hbm, hbm, hbm, vmem, hbm, hbm, hbm],
-        out_specs=(hbm,) * 5,
+        out_specs=(hbm,) * 4,
         scratch_shapes=[
             pltpu.VMEM((SLOTS, height, columns), jnp.float32),
             pltpu.VMEM((units, groups, height, columns), jnp.bfloat16),
@@ -536,15 +674,17 @@
             weight, weight, weight,
             pltpu.VMEM((slots, width), jnp.bfloat16),
             pltpu.VMEM((model_width, slots), jnp.bfloat16),
-            pltpu.VMEM((stack, rows, slots), jnp.bfloat16),
-            pltpu.VMEM((stack - 1, rows, slots), jnp.bfloat16),
-            pltpu.VMEM((stack - 1, rows, slots), jnp.bfloat16),
-            pltpu.VMEM((rows, slots), jnp.bfloat16),
+            pltpu.VMEM((2, stack, rows, slots), jnp.bfloat16),
+            pltpu.VMEM((2, 2, rows, slots), jnp.bfloat16),
+            pltpu.VMEM((2, 2, rows, slots), jnp.bfloat16),
+            pltpu.VMEM((2, rows, slots), jnp.bfloat16),
+            pltpu.VMEM((2, rows, slots), jnp.bfloat16),
+            pltpu.VMEM((2, rows, slots), jnp.bfloat16),
             dma(SLOTS), dma(units, groups - 1), dma(units, groups - 1),
             dma(units, row_groups), dma(units, row_groups),
             dma(row_groups), dma(3), dma(3),
-            dma(stack), dma(stack), dma(stack - 1), dma(stack - 1),
-            dma(groups - 1), dma(groups - 1), dma(2),
+            dma(2, stack), dma(2, stack), dma(2, 2), dma(2, 2), dma(2), dma(2),
+            dma(2, groups - 1), dma(2, groups - 1), dma(2),
         ],
         compiler_params=pltpu.CompilerParams(
             collective_id=collective, has_side_effects=True, vmem_limit_bytes=62 * 1024 * 1024
@@ -553,169 +693,17 @@
             flops=12 * slots * model_width * width, bytes_accessed=32 * sent, transcendentals=0
         ),
     )(gain, gate, up, down, everything, spots, *firsts)
-
-
-def gather_sum_kernel(
-    groups, row_groups, partial_ref, out_ref, own, pair, summed, far, total,
-    load_sem, send_a, recv_a, send_b, recv_b, send_c, recv_c,
-):
-    me = lax.axis_index("tp")
-    row = lax.axis_index("fs")
-    side = lax.rem(row, 2)
-    mate = row + 1 - 2 * side
-    stack = row_groups // 2
-    level = row // 2
-    pieces, slots = total.shape
-    capacity = slots // groups
-
-    barrier = pltpu.get_barrier_semaphore()
-    for step in range(1, groups):
-        pl.semaphore_signal(
-            barrier, inc=1, device_id={"tp": lax.rem(me + step, groups)}, device_id_type=MESH
-        )
-    for step in range(1, row_groups):
-        pl.semaphore_signal(
-            barrier, inc=1, device_id={"fs": lax.rem(row + step, row_groups)}, device_id_type=MESH
-        )
-    order = [stack // 2] + [k for k in range(1, stack) if k != stack // 2] + [0]
-
-    def rows_of(k, which):
-        goal = lax.rem(level + k, stack) * 2 + which
-        return partial_ref.at[pl.ds(pl.multiple_of(goal * pieces, pieces), pieces)]
-
-    def load(k):
-        return pltpu.make_async_copy(rows_of(k, side), own.at[k], load_sem.at[k])
-
-    def across(k):
-        return pltpu.make_async_remote_copy(
-            src_ref=rows_of(k, 1 - side),
-            dst_ref=pair.at[k],
-            send_sem=send_a.at[k],
-            recv_sem=recv_a.at[k],
-            device_id={"fs": mate},
-            device_id_type=MESH,
-        )
-
-    def along(k):
-        return pltpu.make_async_remote_copy(
-            src_ref=summed.at[k],
-            dst_ref=far.at[k],
-            send_sem=send_b.at[k],
-            recv_sem=recv_b.at[k],
-            device_id={"fs": lax.rem(level + k, stack) * 2 + side},
-            device_id_type=MESH,
-        )
-
-    def back(s):
-        goal = lax.rem(me + s, groups)
-        columns = pl.ds(pl.multiple_of(goal * capacity, capacity), capacity)
-        return pltpu.make_async_remote_copy(
-            src_ref=total.at[:, columns],
-            dst_ref=out_ref.at[me],
-            send_sem=send_c.at[s - 1],
-            recv_sem=recv_c.at[s - 1],
-            device_id={"tp": goal},
-            device_id_type=MESH,
-        )
-
-    for k in order:
-        load(k).start()
-    pl.semaphore_wait(barrier, groups - 1 + row_groups - 1)
-    for k in order:
-        across(k).start()
-    strip = 16
-    for k in order:
-        load(k).wait()
-        across(k).wait_recv()
-
-        def add(i, carry):
-            at = pl.ds(pl.multiple_of(i * strip, strip), strip)
-            both = own[k, at, :].astype(jnp.float32) + pair[k, at, :].astype(jnp.float32)
-            summed[k, at, :] = both.astype(jnp.bfloat16)
-            return carry
-
-        if k:
-            lax.fori_loop(0, pieces // strip, add, 0)
-            along(k).start()
-    for k in range(1, stack):
-        along(k).wait_recv()
-
-    def finish(i, carry):
-        at = pl.ds(pl.multiple_of(i * strip, strip), strip)
-        value = own[0, at, :].astype(jnp.float32) + pair[0, at, :].astype(jnp.float32)
-        for k in range(1, stack):
-            value = value + far[k, at, :].astype(jnp.float32)
-        total[at, :] = value.astype(jnp.bfloat16)
-        return carry
-
-    lax.fori_loop(0, pieces // strip, finish, 0)
-    for s in range(1, groups):
-        back(s).start()
-    columns = pl.ds(pl.multiple_of(me * capacity, capacity), capacity)
-    kept = pltpu.make_async_copy(total.at[:, columns], out_ref.at[me], load_sem.at[0])
-    kept.start()
-    kept.wait()
-    for s in range(1, groups):
-        back(s).wait()
-    for k in range(stack):
-        across(k).wait_send()
-        if k:
-            along(k).wait_send()
-
-
-def gather_sum(partial, collective):
-    groups = lax.axis_size("tp")
-    row_groups = lax.axis_size("fs")
-    model_width, slots = partial.shape
-    pieces = model_width // row_groups
-    stack = row_groups // 2
-    capacity = slots // groups
-    block = pltpu.VMEM((stack, pieces, slots), jnp.bfloat16)
-    sent = model_width * slots * 2
-    return pl.pallas_call(
-        functools.partial(gather_sum_kernel, groups, row_groups),
-        out_shape=jax.ShapeDtypeStruct((groups, pieces, capacity), jnp.bfloat16),
-        in_specs=[pl.BlockSpec(memory_space=pl.ANY)],
-        out_specs=pl.BlockSpec(memory_space=pl.ANY),
-        scratch_shapes=[
-            block, block, block, block,
-            pltpu.VMEM((pieces, slots), jnp.bfloat16),
-            pltpu.SemaphoreType.DMA((stack,)),
-            pltpu.SemaphoreType.DMA((stack,)),
-            pltpu.SemaphoreType.DMA((stack,)),
-            pltpu.SemaphoreType.DMA((stack,)),
-            pltpu.SemaphoreType.DMA((stack,)),
-            pltpu.SemaphoreType.DMA((groups - 1,)),
-            pltpu.SemaphoreType.DMA((groups - 1,)),
-        ],
-        compiler_params=pltpu.CompilerParams(
-            collective_id=collective, has_side_effects=True, vmem_limit_bytes=20 * 1024 * 1024
-        ),
-        cost_estimate=pl.CostEstimate(
-            flops=sent, bytes_accessed=32 * sent, transcendentals=0
-        ),
-    )(partial)
 
 
 def fused_device(
     hidden_states, norm_gain, gate_master, up_master, down_master, expert_ids, route_logits
 ):
     groups = lax.axis_size("tp")
-    row_groups = lax.axis_size("fs")
     experts = gate_master.shape[0]
     local_count = experts // groups
     tokens, pieces = hidden_states.shape
-    model_width = pieces * row_groups
     capacity = tokens // 2
-    me = lax.axis_index("tp")
     gain = norm_gain[:, None]
-    id_rows = expert_ids.size // pieces
-    sheet = expert_ids.astype(jnp.bfloat16).reshape(id_rows, pieces)
-    sheet = jnp.pad(sheet, ((0, -id_rows % 16), (0, 0)))
-    everything = lax.all_gather(jnp.concatenate([hidden_states, sheet]), ("fs", "tp"), axis=0)
-    everything = everything.reshape(row_groups, groups, -1, pieces)
-    all_ids = everything[0, :, tokens : tokens + id_rows].astype(jnp.int32)
-    all_ids = all_ids.reshape(groups, tokens, 2)
     earlier = (jnp.arange(tokens)[:, None] > jnp.arange(tokens)[None, :]).astype(jnp.bfloat16)
     weights = jax.nn.softmax(route_logits, axis=1)
     named = expert_ids[:, :, None] == jnp.arange(experts, dtype=jnp.int32)[None, None, :]
@@ -724,19 +712,13 @@
     position = jnp.sum(jnp.where(named, before[:, None, :], 0.0), axis=2).astype(jnp.int32)
     slot_ids = (expert_ids * capacity + position).reshape(-1)
 
-    mine = jnp.any(
-        all_ids[None] == (me * local_count + jnp.arange(local_count))[:, None, None, None], axis=3
+    spots = jnp.where(chosen > 0, before, -1.0).T.reshape(groups, local_count, tokens)
+    *firsts, everything, spots = exchange(
+        gain, gate_master, up_master, down_master, hidden_states, spots, 0, 1
     )
-    spots = jnp.einsum(
-        "ts,jgs->jgt", earlier, mine.astype(jnp.bfloat16), preferred_element_type=jnp.float32
-    ).astype(jnp.int32)
-    spots = jnp.where(mine, spots, -1).reshape(local_count * groups, tokens)
-    firsts = exchange(gain, gate_master, up_master, down_master, hidden_states, 0, 1)
-    gate, up, down, early, partial = serve(
+    gate, up, down, ordered = serve(
         gain, gate_master, up_master, down_master, everything, spots, firsts, 1, 2
     )
-    last = gather_sum(partial, 3)
-    ordered = jnp.stack([early, last], axis=1)
     flat_out = jnp.moveaxis(ordered, 2, 0).reshape(pieces, experts * capacity)
     picked = flat_out.at[:, slot_ids].get(mode="promise_in_bounds")
     picked = picked.reshape(pieces, tokens, 2).astype(jnp.float32)
@@ -766,7 +748,8 @@
     groups = lax.axis_size("tp")
     row_groups = lax.axis_size("fs")
     whole_tiles = gate_master.shape[2] // (row_groups // groups) % 128 == 0
-    if whole_tiles and gate_master.shape[0] == 2 * groups and row_groups % 4 == 0 and expert_ids.size % hidden_states.shape[1] == 0:
+    lined = groups == 4 and row_groups == 8
+    if whole_tiles and lined and gate_master.shape[0] == 2 * groups:
         return fused_device(
             hidden_states, norm_gain, gate_master, up_master, down_master, expert_ids, route_logits
         )

time: 746 us -> 659 us (0.88)
  Pallas kernels: 689 us -> 623 us
  between operations: 14.2 us -> 0.81 us
    pallas_call x1 -> x0, Pallas kernels: 110 us -> none  [gather_sum(): pl.pallas_call(functools.partial(gather_sum_kernel, groups, row_groups),...]
    pallas_call x1, Pallas kernels: 315 us -> 374 us  [serve(): pl.pallas_call(functools.partial(serve_kernel, groups, row_groups, expert...]
    pallas_call x1, Pallas kernels: 264 us -> 250 us  [exchange(): pl.pallas_call(functools.partial(exchange_kernel, groups, row_groups, exp...]
    unnamed x19 -> x21, local copies, waits for them, and re-layouts: 23.6 us -> 22 us
  transfers between devices with their start and end apart: 1 -> 0, of which waited for: 0 -> 0; matrix products, arithmetic and copies ran while one was open for 0% -> 0% of each run, Pallas kernels for 35% -> 0%
where the time goes in v1:
time: 659 us; the launch traced here: 658 us
  Pallas kernels  623 us (95%)
  local copies, waits for them, and re-layouts  29.6 us (4%)
    pallas_call x1, Pallas kernels, serve(): pl.pallas_call(functools.partial(serve_kernel, groups, row_groups, expert...  374 us
    pallas_call x1, Pallas kernels, exchange(): pl.pallas_call(functools.partial(exchange_kernel, groups, row_groups, exp...  250 us
    unnamed x21, local copies, waits for them, and re-layouts  22 us

profile of v1, /device:TPU:0, one launch (start us, length us, event | category | flops | bytes accessed | tf_op | source)
XLA Modules:
  0.0 658.4 jit_solution(9942538080234597593)
XLA Ops:
  0.6 0.7 fusion.1
  1.3 0.2 fusion
  1.6 0.8 copy.22.gain_ref
  2.4 0.0 copy-start.1
  2.4 0.9 copy-done.1
  3.4 0.0 copy-start
  3.4 249.7 %shard_map.102 = (bf16[2048,896]{1,0:T(8,128)(2,1)S(1)}, bf16[2048,896]{1,0:T(8,128)(2,1)S(1)}, bf16[2048,896]{1,0:T(8,128)(2,1)}, bf16[8,4,512,256]{3,2,1,0:T(8,128)(2,1)}, f32[4,2,512]{2,1,0:T(2,128)S(1)}) custom-call(f32[256,1]{1,0:T(8,128)S(1)} %copy.22.gain_ref, f32[8,256,1792]{2,1,0:T(8,128)} %gate_ref.3, f32[8,256,1792]{2,1,0:T(8,128)} %up_ref.3, ...), custom_call_target="tpu_custom_call" | custom-call | flops 458752 | bytes 352321536 | tf_op jit(solution)/shard_map/pallas_call | solution.py:251
  253.1 0.0 copy-done
  253.1 0.0 copy-start.2
  253.1 1.8 copy-done.2
  254.9 0.0 copy-start.3
  254.9 1.8 copy-done.3
  256.8 0.0 copy-start.4
  256.8 0.6 copy-done.4
  257.4 0.0 copy-start.6
  257.4 373.6 %shard_map.103 = (bf16[2,2048,896]{2,1,0:T(8,128)(2,1)}, bf16[2,2048,896]{2,1,0:T(8,128)(2,1)}, bf16[2,2048,896]{2,1,0:T(8,128)(2,1)}, bf16[4,2,256,256]{3,2,1,0:T(8,128)(2,1)}) custom-call(f32[256,1]{1,0:T(8,128)} %copy-done, f32[8,256,1792]{2,1,0:T(8,128)} %gate_ref.3, f32[8,256,1792]{2,1,0:T(8,128)} %up_ref.3, f32[8,256,1792]{2,1,0:T(8,128)} %down_ref.3, ...), custom_call_target="tpu_custom_call" | custom-call | flops 22548578304 | bytes 352321536 | tf_op jit(solution)/shard_map/pallas_call | solution.py:660
  631.0 0.0 copy-start.5
  631.0 1.5 copy.23
  632.5 0.0 copy-done.6
  632.6 0.1 copy.24
  632.7 0.2 reshape.55
  632.9 4.1 gather_fusion
  637.1 0.1 convert_bitcast_fusion
  637.1 0.6 reshape.56
  637.8 0.0 copy-done.5
  637.9 0.1 copy.25
  638.0 3.6 multiply_reduce_fusion
  641.6 0.0 slice-start
  641.6 6.9 %copy.29 = bf16[2,2048,896]{2,1,0:T(8,128)(2,1)} copy(bf16[2,2048,896]{2,1,0:T(8,128)(2,1)} %get-tuple-element.26) | data formatting | bytes 14680064
  648.5 0.0 slice-start.1
  648.5 6.9 %copy.30 = bf16[2,2048,896]{2,1,0:T(8,128)(2,1)} copy(bf16[2,2048,896]{2,1,0:T(8,128)(2,1)} %get-tuple-element.27) | data formatting | bytes 14680064
  655.3 0.0 slice-done
  655.3 0.0 slice-done.1
  655.3 3.0 copy.31
  (10 shorter events, 0.2 us)
Async XLA Ops:
  2.4 1.0 copy-start.1
  3.4 249.7 %copy-start = (f32[256,1]{1,0:T(8,128)}, f32[256,1]{1,0:T(8,128)S(1)}, u32[]{:S(2)}) copy-start(f32[256,1]{1,0:T(8,128)S(1)} %copy.22.gain_ref) | copy-start | bytes 3076
  253.1 1.8 copy-start.2
  254.9 1.8 copy-start.3
  256.8 0.6 copy-start.4
  257.4 375.1 %copy-start.6 = (s32[512,2]{0,1:T(2,128)S(1)}, s32[512,2]{0,1:T(2,128)}, u32[]{:S(2)}) copy-start(s32[512,2]{0,1:T(2,128)} %param.12) | copy-start | bytes 12292
  631.0 6.8 %copy-start.5 = (f32[512,2]{0,1:T(2,128)S(1)}, f32[512,2]{0,1:T(2,128)}, u32[]{:S(2)}) copy-start(f32[512,2]{0,1:T(2,128)} %param.13) | copy-start | bytes 12292
  641.6 13.7 %slice-start = ((s8[7340032]{0:T(1024)(128)(4,1)}), s8[4194304]{0:T(1024)(128)(4,1)S(1)}, s32[]{:S(2)}) async-start(s8[7340032]{0:T(1024)(128)(4,1)} %bitcast.15), calls=%async_computation | async-start | bytes 8388608
  648.5 6.9 %slice-start.1 = ((s8[7340032]{0:T(1024)(128)(4,1)}), s8[3145728]{0:T(1024)(128)(4,1)S(1)}, s32[]{:S(2)}) async-start(s8[7340032]{0:T(1024)(128)(4,1)} %bitcast.15), calls=%async_computation.1 | async-start | bytes 6291456

commit v2 on v1

--- a/solution.py
+++ b/solution.py
@@ -37,9 +37,11 @@
         pl.semaphore_signal(
             barrier, inc=1, device_id={"fs": lax.rem(row + step, row_groups)}, device_id_type=MESH
         )
-    order = [groups // 2] + [s for s in range(1, groups) if s != groups // 2] + [0]
+    rest = [s for s in range(1, groups) if s != groups // 2]
+    order = [groups // 2] + rest + [0]
+    opening = [groups // 2, 0] + rest
     units = [(w, c) for w in range(len(masters)) for c in range(chunks)]
-    jobs = [(u, s) for u in range(len(units)) for s in order]
+    jobs = [(u, s) for u in range(len(units)) for s in (order if u else opening)]
 
     def load(n):
         u, s = jobs[n]
@@ -199,12 +201,13 @@
             load(n + SLOTS).start()
         if s == 0:
             pass_on(u, 0)
+        else:
+            first(u, s).start()
+        if n + 1 == len(jobs) or jobs[n + 1][0] != u:
             if u >= 1:
                 forward(u - 1)
             if u in tasks:
                 tasks[u]()
-        else:
-            first(u, s).start()
     forward(len(units) - 1)
     own_kept.wait()
     spot_kept.wait()
@@ -268,7 +271,7 @@
             dma(groups - 1), dma(groups - 1), dma(2),
         ],
         compiler_params=pltpu.CompilerParams(
-            collective_id=collective, has_side_effects=True, vmem_limit_bytes=44 * 1024 * 1024
+            collective_id=collective, has_side_effects=True, vmem_limit_bytes=62 * 1024 * 1024
         ),
         cost_estimate=pl.CostEstimate(
             flops=rows * columns, bytes_accessed=32 * sent, transcendentals=0
@@ -313,9 +316,11 @@
         pl.semaphore_signal(
             barrier, inc=1, device_id={"fs": lax.rem(row + step, row_groups)}, device_id_type=MESH
         )
-    order = [groups // 2] + [s for s in range(1, groups) if s != groups // 2] + [0]
+    rest = [s for s in range(1, groups) if s != groups // 2]
+    order = [groups // 2] + rest + [0]
+    opening = [groups // 2, 0] + rest
     units = [(w, c) for w in range(len(masters)) for c in range(chunks)]
-    jobs = [(u, s) for u in range(len(units)) for s in order]
+    jobs = [(u, s) for u in range(len(units)) for s in (order if u else opening)]
 
     def load(n):
         u, s = jobs[n]
@@ -419,8 +424,8 @@
 
         lax.fori_loop(0, groups, one, 0)
 
-    def lower(r):
-        at = pl.ds(pl.multiple_of(r * rows, rows), rows)
+    def lower(start, size):
+        at = pl.ds(pl.multiple_of(start, size), size)
         partial[at, :] = lax.dot_general(
             down_w[at, :], act[...], (((1,), (1,)), ((), ())), preferred_element_type=jnp.float32
         ).astype(jnp.bfloat16)
@@ -435,88 +440,91 @@
     def level_at(d):
         return lax.rem(level // 2 + d // 2, 2) * 2 + lax.rem(level + d, 2)
 
-    def across(j, d):
-        goal = level_at(d) * 2 + 1 - side
+    def span(c):
+        return pl.ds(c * height, height)
+
+    def across(j, d, c):
+        start = (level_at(d) * 2 + 1 - side) * rows + c * height
         return pltpu.make_async_remote_copy(
-            src_ref=partial.at[pl.ds(pl.multiple_of(goal * rows, rows), rows)],
-            dst_ref=pair.at[j, d],
-            send_sem=send_c.at[j, d],
-            recv_sem=recv_c.at[j, d],
+            src_ref=partial.at[pl.ds(pl.multiple_of(start, height), height)],
+            dst_ref=pair.at[j, d, span(c)],
+            send_sem=send_c.at[j, d, c],
+            recv_sem=recv_c.at[j, d, c],
             device_id={"fs": mate},
             device_id_type=MESH,
         )
 
-    def along_near(j, d):
+    def along_near(j, d, c):
         return pltpu.make_async_remote_copy(
-            src_ref=to_near.at[j, d - 1],
-            dst_ref=near.at[j, d - 1],
-            send_sem=send_d.at[j, d - 1],
-            recv_sem=recv_d.at[j, d - 1],
+            src_ref=to_near.at[j, d - 1, span(c)],
+            dst_ref=near.at[j, d - 1, span(c)],
+            send_sem=send_d.at[j, d - 1, c],
+            recv_sem=recv_d.at[j, d - 1, c],
             device_id={"fs": level_at(1) * 2 + side},
             device_id_type=MESH,
         )
 
-    def along_far(j):
+    def along_far(j, c):
         return pltpu.make_async_remote_copy(
-            src_ref=to_far.at[j],
-            dst_ref=far.at[j],
-            send_sem=send_f.at[j],
-            recv_sem=recv_f.at[j],
+            src_ref=to_far.at[j, span(c)],
+            dst_ref=far.at[j, span(c)],
+            send_sem=send_f.at[j, c],
+            recv_sem=recv_f.at[j, c],
             device_id={"fs": level_at(3) * 2 + side},
             device_id_type=MESH,
         )
 
-    def back(j, s):
+    def back(j, s, c):
         goal = lax.rem(me + s, groups)
+        columns = pl.ds(pl.multiple_of(goal * capacity, capacity), capacity)
         return pltpu.make_async_remote_copy(
-            src_ref=total.at[j, :, pl.ds(pl.multiple_of(goal * capacity, capacity), capacity)],
-            dst_ref=back_out.at[me, j],
-            send_sem=send_e.at[j, s - 1],
-            recv_sem=recv_e.at[j, s - 1],
+            src_ref=total.at[j, span(c), columns],
+            dst_ref=back_out.at[me, j, span(c)],
+            send_sem=send_e.at[j, s - 1, c],
+            recv_sem=recv_e.at[j, s - 1, c],
             device_id={"tp": goal},
             device_id_type=MESH,
         )
 
-    def kept(j):
+    def kept(j, c):
+        columns = pl.ds(pl.multiple_of(me * capacity, capacity), capacity)
         return pltpu.make_async_copy(
-            total.at[j, :, pl.ds(pl.multiple_of(me * capacity, capacity), capacity)],
-            back_out.at[me, j],
-            last_sem.at[j],
-        )
-
-    def sum_into(j, d, target, others):
+            total.at[j, span(c), columns], back_out.at[me, j, span(c)], last_sem.at[j, c]
+        )
+
+    def sum_into(j, d, c, target, others):
         base = (level_at(d) * 2 + side) * rows
 
         def add(i, carry):
-            at = pl.ds(pl.multiple_of(i * strip, strip), strip)
-            mine = pl.ds(pl.multiple_of(base + i * strip, strip), strip)
+            at = pl.ds(pl.multiple_of(c * height + i * strip, strip), strip)
+            mine = pl.ds(pl.multiple_of(base + c * height + i * strip, strip), strip)
             value = partial[mine, :].astype(jnp.float32) + pair[j, d, at, :].astype(jnp.float32)
             for other in others:
                 value = value + other[at, :].astype(jnp.float32)
             target[at, :] = value.astype(jnp.bfloat16)
             return carry
 
-        lax.fori_loop(0, rows // strip, add, 0)
-
-    def to_level(j, d):
-        across(j, d).wait_recv()
-        sum_into(j, d, to_near.at[j, d - 1], ())
-        along_near(j, d).start()
-
-    def cross_over(j):
-        across(j, 3).wait_recv()
-        along_near(j, 2).wait_recv()
-        sum_into(j, 3, to_far.at[j], (near.at[j, 1],))
-        along_far(j).start()
-
-    def settle_sum(j):
-        across(j, 0).wait_recv()
-        along_near(j, 1).wait_recv()
-        along_far(j).wait_recv()
-        sum_into(j, 0, total.at[j], (near.at[j, 0], far.at[j]))
+        lax.fori_loop(0, height // strip, add, 0)
+
+    def to_level(j, d, c):
+        across(j, d, c).wait_recv()
+        sum_into(j, d, c, to_near.at[j, d - 1], ())
+        along_near(j, d, c).start()
+
+    def cross_over(j, c):
+        across(j, 3, c).wait_recv()
+        along_near(j, 2, c).wait_recv()
+        sum_into(j, 3, c, to_far.at[j], (near.at[j, 1],))
+        along_far(j, c).start()
+
+    def settle_sum(j, c):
+        across(j, 0, c).wait_recv()
+        along_near(j, 1, c).wait_recv()
+        along_far(j, c).wait_recv()
+        sum_into(j, 0, c, total.at[j], (near.at[j, 0], far.at[j]))
         for s in range(1, groups):
-            back(j, s).start()
-        kept(j).start()
+            back(j, s, c).start()
+        kept(j, c).start()
 
     def after_0():
         for w in range(len(masters)):
@@ -534,19 +542,22 @@
         keep(2).start()
 
         def one(r, carry):
-            lower(r)
+            lower(r * rows, rows)
             return carry
 
         lax.fori_loop(0, row_groups, one, 0)
-        for d in range(stack):
-            across(0, d).start()
+        for c in range(chunks):
+            for d in range(stack):
+                across(0, d, c).start()
 
     def after_3():
-        to_level(0, 1)
-        to_level(0, 2)
+        for c in range(chunks):
+            to_level(0, 2, c)
+            to_level(0, 1, c)
 
     def after_4():
-        cross_over(0)
+        for c in range(chunks):
+            cross_over(0, c)
 
     tasks = {0: after_0, 1: after_1, 2: after_2, 3: after_3, 4: after_4}
 
@@ -569,17 +580,19 @@
             load(n + SLOTS).start()
         if s == 0:
             pass_on(u, 0)
+        else:
+            first(u, s).start()
+        if n + 1 == len(jobs) or jobs[n + 1][0] != u:
             if u >= 1:
                 forward(u - 1)
             if u in tasks:
                 tasks[u]()
-        else:
-            first(u, s).start()
     forward(len(units) - 1)
     pack(1)
-    settle_sum(0)
-    for d in range(stack):
-        across(0, d).wait_send()
+    for c in range(chunks):
+        settle_sum(0, c)
+        for d in range(stack):
+            across(0, d, c).wait_send()
     for w in range(2):
         keep(w).wait()
         for c in range(chunks):
@@ -591,40 +604,50 @@
     hidden()
     keep(2).wait()
 
-    def piece(d, i):
-        r = level_at(d) * 2 + lax.rem(side + 1 + i, 2)
-        at = pl.ds(pl.multiple_of(r * rows, rows), rows)
+    def piece(d, i, c):
+        source = level_at(d) * 2 + lax.rem(side + 1 + i, 2)
+        at = pl.ds(pl.multiple_of(source * rows + c * height, height), height)
         copy = pltpu.make_async_copy(outs[2].at[expert, at], down_w.at[at], raw_sem.at[i])
-        return r, copy
-
-    for d in range(stack):
+        return source, copy
+
+    def level_product(d, c):
         for i in range(2):
-            r, copy = piece(d, i)
-            for c in range(chunks):
-                arrived(2 * chunks + c, r)
+            source, copy = piece(d, i, c)
+            arrived(2 * chunks + c, source)
             copy.start()
         for i in range(2):
-            piece(d, i)[1].wait()
+            piece(d, i, c)[1].wait()
 
         def one(i, carry):
-            lower(level_at(d) * 2 + lax.rem(side + 1 + i, 2))
+            lower((level_at(d) * 2 + lax.rem(side + 1 + i, 2)) * rows + c * height, height)
             return carry
 
         lax.fori_loop(0, 2, one, 0)
-        across(1, d).start()
-        if d >= 2:
-            to_level(1, d - 1)
-    cross_over(1)
-    settle_sum(1)
-    for d in range(stack):
-        across(1, d).wait_send()
-    for j in range(2):
-        for d in (1, 2):
-            along_near(j, d).wait_send()
-        along_far(j).wait_send()
-        kept(j).wait()
-        for s in range(1, groups):
-            back(j, s).wait()
+        across(1, d, c).start()
+
+    for c in range(chunks):
+        for d in range(stack):
+            if c and d == 2:
+                to_level(1, 2, c - 1)
+                to_level(1, 1, c - 1)
+            level_product(d, c)
+        if c:
+            cross_over(1, c - 1)
+    to_level(1, 2, chunks - 1)
+    to_level(1, 1, chunks - 1)
+    cross_over(1, chunks - 1)
+    for c in range(chunks):
+        settle_sum(1, c)
+    for c in range(chunks):
+        for d in range(stack):
+            across(1, d, c).wait_send()
+        for j in range(2):
+            for d in (1, 2):
+                along_near(j, d, c).wait_send()
+            along_far(j, c).wait_send()
+            kept(j, c).wait()
+            for s in range(1, groups):
+                back(j, s, c).wait()
     for u in range(len(units)):
         for s in range(groups):
             if s:
@@ -683,8 +706,9 @@
             dma(SLOTS), dma(units, groups - 1), dma(units, groups - 1),
             dma(units, row_groups), dma(units, row_groups),
             dma(row_groups), dma(3), dma(3),
-            dma(2, stack), dma(2, stack), dma(2, 2), dma(2, 2), dma(2), dma(2),
-            dma(2, groups - 1), dma(2, groups - 1), dma(2),
+            dma(2, stack, chunks), dma(2, stack, chunks),
+            dma(2, 2, chunks), dma(2, 2, chunks), dma(2, chunks), dma(2, chunks),
+            dma(2, groups - 1, chunks), dma(2, groups - 1, chunks), dma(2, chunks),
         ],
         compiler_params=pltpu.CompilerParams(
             collective_id=collective, has_side_effects=True, vmem_limit_bytes=62 * 1024 * 1024
@@ -693,6 +717,84 @@
             flops=12 * slots * model_width * width, bytes_accessed=32 * sent, transcendentals=0
         ),
     )(gain, gate, up, down, everything, spots, *firsts)
+
+
+def finish_kernel(
+    parts, gate_ref, up_ref, down_ref, back_ref, slot_ref, logit_ref,
+    gate_out, up_out, down_out, out_ref, held, load_sem, store_sem,
+):
+    sources = (gate_ref, up_ref, down_ref)
+    goals = (gate_out, up_out, down_out)
+    local_count, height, width = gate_ref.shape
+    part = height // parts
+    pieces = [
+        (w, j, pl.ds(p * part, part))
+        for w in range(3) for j in range(local_count) for p in range(parts)
+    ]
+
+    def load(n):
+        w, j, at = pieces[n]
+        return pltpu.make_async_copy(sources[w].at[j, at], held.at[n], load_sem.at[n])
+
+    def store(n):
+        w, j, at = pieces[n]
+        return pltpu.make_async_copy(held.at[n], goals[w].at[j, at], store_sem.at[n])
+
+    for n in range(len(pieces)):
+        load(n).start()
+    tokens, features = out_ref.shape
+    groups, count, _, capacity = back_ref.shape
+    logits = logit_ref[...]
+    scores = [logits[:, k : k + 1] for k in range(2)]
+    largest = jnp.maximum(scores[0], scores[1])
+    powers = [jnp.exp(score - largest) for score in scores]
+    whole = powers[0] + powers[1]
+    slots = slot_ref[...]
+    value = jnp.zeros((tokens, features), jnp.float32)
+    done = 0
+    for e in range(groups * count):
+        block = back_ref[e // count, e % count]
+        names = lax.broadcasted_iota(jnp.int32, (tokens, capacity), 1) + e * capacity
+        for k in range(2):
+            table = jnp.where(names == slots[:, k : k + 1], 1.0, 0.0).astype(jnp.bfloat16)
+            picked = lax.dot_general(
+                table, block, (((1,), (1,)), ((), ())), preferred_element_type=jnp.float32
+            )
+            value = value + picked * (powers[k] / whole)
+        until = (e + 1) * len(pieces) // (groups * count)
+        for n in range(done, until):
+            load(n).wait()
+            store(n).start()
+        done = until
+    out_ref[...] = value.astype(jnp.bfloat16)
+    for n in range(len(pieces)):
+        store(n).wait()
+
+
+def finish(gate, up, down, back, slots, logits, features):
+    parts = 4
+    local_count, height, width = gate.shape
+    count = 3 * local_count * parts
+    hbm = pl.BlockSpec(memory_space=pl.ANY)
+    vmem = pl.BlockSpec(memory_space=pltpu.VMEM)
+    same = jax.ShapeDtypeStruct(gate.shape, gate.dtype)
+    return pl.pallas_call(
+        functools.partial(finish_kernel, parts),
+        out_shape=(
+            same, same, same, jax.ShapeDtypeStruct((slots.shape[0], features), jnp.bfloat16)
+        ),
+        in_specs=[hbm, hbm, hbm, vmem, vmem, vmem],
+        out_specs=(hbm, hbm, hbm, vmem),
+        scratch_shapes=[
+            pltpu.VMEM((count, height // parts, width), jnp.bfloat16),
+            pltpu.SemaphoreType.DMA((count,)),
+            pltpu.SemaphoreType.DMA((count,)),
+        ],
+        compiler_params=pltpu.CompilerParams(vmem_limit_bytes=56 * 1024 * 1024),
+        cost_estimate=pl.CostEstimate(
+            flops=4 * slots.shape[0] * back.size, bytes_accessed=12 * gate.size, transcendentals=0
+        ),
+    )(gate, up, down, back, slots, logits)
 
 
 def fused_device(
@@ -705,13 +807,11 @@
     capacity = tokens // 2
     gain = norm_gain[:, None]
     earlier = (jnp.arange(tokens)[:, None] > jnp.arange(tokens)[None, :]).astype(jnp.bfloat16)
-    weights = jax.nn.softmax(route_logits, axis=1)
     named = expert_ids[:, :, None] == jnp.arange(experts, dtype=jnp.int32)[None, None, :]
     chosen = jnp.any(named, axis=1).astype(jnp.bfloat16)
     before = jnp.dot(earlier, chosen, preferred_element_type=jnp.float32)
     position = jnp.sum(jnp.where(named, before[:, None, :], 0.0), axis=2).astype(jnp.int32)
-    slot_ids = (expert_ids * capacity + position).reshape(-1)
-
+    slot_ids = expert_ids * capacity + position
     spots = jnp.where(chosen > 0, before, -1.0).T.reshape(groups, local_count, tokens)
     *firsts, everything, spots = exchange(
         gain, gate_master, up_master, down_master, hidden_states, spots, 0, 1
@@ -719,11 +819,7 @@
     gate, up, down, ordered = serve(
         gain, gate_master, up_master, down_master, everything, spots, firsts, 1, 2
     )
-    flat_out = jnp.moveaxis(ordered, 2, 0).reshape(pieces, experts * capacity)
-    picked = flat_out.at[:, slot_ids].get(mode="promise_in_bounds")
-    picked = picked.reshape(pieces, tokens, 2).astype(jnp.float32)
-    combined = jnp.sum(picked * weights[None, :, :], axis=2)
-    return gate, up, down, jnp.transpose(combined).astype(jnp.bfloat16)
+    return finish(gate, up, down, ordered, slot_ids, route_logits, pieces)
 
 
 def arrange(weights, groups, row_groups):

time: 659 us -> 637 us (0.967)
  local copies, waits for them, and re-layouts: 29.6 us -> 4.51 us
    unnamed x21 -> x1, local copies, waits for them, and re-layouts: 22 us -> 1.56 us
    pallas_call x0 -> x1, Pallas kernels: none -> 17.5 us  [finish(): pl.pallas_call(functools.partial(finish_kernel, parts), out_shape=(same,...]
    pallas_call x1, Pallas kernels: 374 us -> 361 us  [serve(): pl.pallas_call(functools.partial(serve_kernel, groups, row_groups, expert...]
where the time goes in v2:
time: 637 us
  Pallas kernels  629 us (99%)
    pallas_call x1, Pallas kernels, serve(): pl.pallas_call(functools.partial(serve_kernel, groups, row_groups, expert...  361 us
    pallas_call x1, Pallas kernels, exchange(): pl.pallas_call(functools.partial(exchange_kernel, groups, row_groups, exp...  251 us
    pallas_call x1, Pallas kernels, finish(): pl.pallas_call(functools.partial(finish_kernel, parts), out_shape=(same,...  17.5 us

profile of v2, /device:TPU:0, one launch (start us, length us, event | category | flops | bytes accessed | tf_op | source)
XLA Modules:
  0.0 636.6 jit_solution(13567880388094011177)
XLA Ops:
  0.6 0.7 fusion.1
  1.3 0.2 fusion
  1.6 0.7 select_reduce_fusion
  2.3 0.6 reshape.13.spot_ref
  2.9 0.7 convert_add_fusion
  3.6 1.5 copy.30.gain_ref
  5.1 0.9 copy.31.slot_ref
  5.9 1.6 copy.32.logit_ref
  7.5 250.7 %shard_map.102 = (bf16[2048,896]{1,0:T(8,128)(2,1)}, bf16[2048,896]{1,0:T(8,128)(2,1)}, bf16[2048,896]{1,0:T(8,128)(2,1)}, bf16[8,4,512,256]{3,2,1,0:T(8,128)(2,1)}, f32[4,2,512]{2,1,0:T(2,128)}) custom-call(f32[256,1]{1,0:T(8,128)} %copy.30.gain_ref, f32[8,256,1792]{2,1,0:T(8,128)} %gate_ref.3, f32[8,256,1792]{2,1,0:T(8,128)} %up_ref.3, ...), custom_call_target="tpu_custom_call" | custom-call | flops 458752 | bytes 352321536 | tf_op jit(solution)/shard_map/pallas_call | solution.py:254
  258.2 360.8 %shard_map.103 = (bf16[2,2048,896]{2,1,0:T(8,128)(2,1)}, bf16[2,2048,896]{2,1,0:T(8,128)(2,1)}, bf16[2,2048,896]{2,1,0:T(8,128)(2,1)}, bf16[4,2,256,256]{3,2,1,0:T(8,128)(2,1)}) custom-call(f32[256,1]{1,0:T(8,128)} %copy.30.gain_ref, f32[8,256,1792]{2,1,0:T(8,128)} %gate_ref.3, f32[8,256,1792]{2,1,0:T(8,128)} %up_ref.3, f32[8,256,1792]{2,1,0:T(8,128)} %down_ref.3, ...), custom_call_target="tpu_custom_call" | custom-call | flops 22548578304 | bytes 352321536 | tf_op jit(solution)/shard_map/pallas_call | solution.py:683
  619.0 17.5 %shard_map.104 = (bf16[2,2048,896]{2,1,0:T(8,128)(2,1)}, bf16[2,2048,896]{2,1,0:T(8,128)(2,1)}, bf16[2,2048,896]{2,1,0:T(8,128)(2,1)}, bf16[512,256]{1,0:T(8,128)(2,1)}) custom-call(bf16[2,2048,896]{2,1,0:T(8,128)(2,1)} %get-tuple-element.18.gate_ref, bf16[2,2048,896]{2,1,0:T(8,128)(2,1)} %get-tuple-element.19.up_ref, ...), custom_call_target="tpu_custom_call" | custom-call | flops 1073741824 | bytes 44040192 | tf_op jit(solution)/shard_map/pallas_call | solution.py:781
  (1 shorter events, 0.0 us)

commit v3 on v2

--- a/solution.py
+++ b/solution.py
@@ -13,7 +13,7 @@
 
 
 def exchange_kernel(
-    groups, row_groups, expert, chunks, gain_ref, gate_ref, up_ref, down_ref, own_ref, spot_ref,
+    groups, row_groups, expert, units, gain_ref, gate_ref, up_ref, down_ref, own_ref, spot_ref,
     gate_out, up_out, down_out, all_out, spot_out, stage, cast, landed, load_sem,
     send_a, recv_a, send_b, recv_b, send_z, recv_z, send_y, recv_y, send_t, recv_t,
     send_s, recv_s, own_sem,
@@ -25,8 +25,8 @@
     outs = (gate_out, up_out, down_out)
     local_count = gate_ref.shape[0] // groups
     rows, columns = gate_ref.shape[1:]
-    height = rows // chunks
     width = columns // blocks
+    strip = 16
 
     barrier = pltpu.get_barrier_semaphore()
     for step in range(1, groups):
@@ -40,16 +40,15 @@
     rest = [s for s in range(1, groups) if s != groups // 2]
     order = [groups // 2] + rest + [0]
     opening = [groups // 2, 0] + rest
-    units = [(w, c) for w in range(len(masters)) for c in range(chunks)]
     jobs = [(u, s) for u in range(len(units)) for s in (order if u else opening)]
 
     def load(n):
         u, s = jobs[n]
-        w, c = units[u]
+        w, start, size = units[u]
         number = lax.rem(me + s, groups) * local_count + expert
         return pltpu.make_async_copy(
-            masters[w].at[number, pl.ds(c * height, height)],
-            stage.at[n % SLOTS],
+            masters[w].at[number, pl.ds(start, size)],
+            stage.at[n % SLOTS, pl.ds(0, size)],
             load_sem.at[n % SLOTS],
         )
 
@@ -57,10 +56,18 @@
         load(n).start()
     pl.semaphore_wait(barrier, groups - 1 + row_groups - 1)
 
+    def cast_at(u, s):
+        w, start, size = units[u]
+        return cast.at[w, s, pl.ds(start, size)]
+
+    def landed_at(u, s):
+        w, start, size = units[u]
+        return landed.at[w, s - 1, pl.ds(start, size)]
+
     def first(u, s):
         return pltpu.make_async_remote_copy(
-            src_ref=cast.at[u, s],
-            dst_ref=landed.at[u, s - 1],
+            src_ref=cast_at(u, s),
+            dst_ref=landed_at(u, s),
             send_sem=send_a.at[u, s - 1],
             recv_sem=recv_a.at[u, s - 1],
             device_id={"tp": lax.rem(me + s, groups)},
@@ -68,12 +75,12 @@
         )
 
     def place(u, source):
-        w, c = units[u]
-        start = pl.multiple_of(source * rows + c * height, height)
-        return outs[w].at[pl.ds(start, height)]
+        w, start, size = units[u]
+        at = pl.ds(pl.multiple_of(source * rows + start, strip), size)
+        return outs[w].at[at]
 
     def second(u, s, b):
-        held = cast.at[u, 0] if s == 0 else landed.at[u, s - 1]
+        held = landed_at(u, s) if s else cast_at(u, 0)
         goal = lax.rem(me + groups - s, groups) * blocks + b
         piece = held.at[:, pl.ds(b * width, width)]
         remote = lambda: pltpu.make_async_remote_copy(
@@ -180,10 +187,9 @@
             for s in range(1, groups):
                 over_tp(k, 1, s).start()
 
-    tasks = {1: near_blocks, 3: far_blocks}
-    strip = 16
+    tasks = {2: near_blocks, 4: far_blocks}
     for n, (u, s) in enumerate(jobs):
-        w, c = units[u]
+        w, start, size = units[u]
         load(n).wait()
         slot = n % SLOTS
 
@@ -191,12 +197,13 @@
             at = pl.ds(pl.multiple_of(i * strip, strip), strip)
             value = stage[slot, at, :]
             if w < 2:
-                gain = gain_ref[pl.ds(pl.multiple_of(c * height + i * strip, strip), strip), :]
+                gain = gain_ref[pl.ds(pl.multiple_of(start + i * strip, strip), strip), :]
                 value = value * gain
-            cast[u, s, at, :] = value.astype(jnp.bfloat16)
+            to = pl.ds(pl.multiple_of(start + i * strip, strip), strip)
+            cast[w, s, to, :] = value.astype(jnp.bfloat16)
             return carry
 
-        lax.fori_loop(0, height // strip, convert, 0)
+        lax.fori_loop(0, size // strip, convert, 0)
         if n + SLOTS < len(jobs):
             load(n + SLOTS).start()
         if s == 0:
@@ -232,7 +239,7 @@
                     remote().wait_send()
         for source in range(row_groups):
             pltpu.make_async_copy(
-                cast.at[u, 0, :, pl.ds(0, width)], place(u, source), recv_b.at[u, source]
+                cast_at(u, 0).at[:, pl.ds(0, width)], place(u, source), recv_b.at[u, source]
             ).wait()
 
 
@@ -242,9 +249,11 @@
     experts, rows, columns = gate.shape
     blocks = row_groups // groups
     width = columns // blocks
-    chunks = 2
-    units = 3 * chunks
-    height = rows // chunks
+    eighth = rows // 8
+    plan = [(0, 0, eighth), (0, eighth, 3 * eighth), (0, 4 * eighth, 4 * eighth)]
+    plan += [(w, start, 4 * eighth) for w in (1, 2) for start in (0, 4 * eighth)]
+    units = len(plan)
+    height = 4 * eighth
     out = jax.ShapeDtypeStruct((rows * row_groups, width), jnp.bfloat16)
     hbm = pl.BlockSpec(memory_space=pl.ANY)
     stack = row_groups // 2
@@ -252,7 +261,7 @@
     sent = 3 * rows * columns * 2 * groups
     dma = lambda *shape: pltpu.SemaphoreType.DMA(shape)
     return pl.pallas_call(
-        functools.partial(exchange_kernel, groups, row_groups, expert, chunks),
+        functools.partial(exchange_kernel, groups, row_groups, expert, plan),
         out_shape=(
             out, out, out,
             jax.ShapeDtypeStruct((row_groups, groups) + hidden.shape, hidden.dtype),
@@ -262,8 +271,8 @@
         out_specs=(hbm,) * 5,
         scratch_shapes=[
             pltpu.VMEM((SLOTS, height, columns), jnp.float32),
-            pltpu.VMEM((units, groups, height, columns), jnp.bfloat16),
-            pltpu.VMEM((units, groups - 1, height, columns), jnp.bfloat16),
+            pltpu.VMEM((3, groups, rows, columns), jnp.bfloat16),
+            pltpu.VMEM((3, groups - 1, rows, columns), jnp.bfloat16),
             dma(SLOTS), dma(units, groups - 1), dma(units, groups - 1),
             dma(units, row_groups), dma(units, row_groups),
             dma(stack - 1), dma(stack - 1), dma(stack), dma(stack),
@@ -280,7 +289,7 @@
 
 
 def serve_kernel(
-    groups, row_groups, expert, chunks, gain_ref, gate_ref, up_ref, down_ref, all_ref, spot_ref,
+    groups, row_groups, expert, units, gain_ref, gate_ref, up_ref, down_ref, all_ref, spot_ref,
     gate_first, up_first, down_first,
     gate_out, up_out, down_out, back_out,
     stage, cast, landed, raw, rows_in, gate_w, up_w, down_w, act, partial,
@@ -297,7 +306,6 @@
     held_w = (gate_w, up_w, down_w)
     local_count = gate_ref.shape[0] // groups
     rows, columns = gate_ref.shape[1:]
-    height = rows // chunks
     width = columns // blocks
     tokens, model_width = raw.shape
     capacity = tokens // 2
@@ -319,16 +327,15 @@
     rest = [s for s in range(1, groups) if s != groups // 2]
     order = [groups // 2] + rest + [0]
     opening = [groups // 2, 0] + rest
-    units = [(w, c) for w in range(len(masters)) for c in range(chunks)]
     jobs = [(u, s) for u in range(len(units)) for s in (order if u else opening)]
 
     def load(n):
         u, s = jobs[n]
-        w, c = units[u]
+        w, start, size = units[u]
         number = lax.rem(me + s, groups) * local_count + expert
         return pltpu.make_async_copy(
-            masters[w].at[number, pl.ds(c * height, height)],
-            stage.at[n % SLOTS],
+            masters[w].at[number, pl.ds(start, size)],
+            stage.at[n % SLOTS, pl.ds(0, size)],
             load_sem.at[n % SLOTS],
         )
 
@@ -336,10 +343,18 @@
         load(n).start()
     pl.semaphore_wait(barrier, groups - 1 + row_groups - 1)
 
+    def cast_at(u, s):
+        w, start, size = units[u]
+        return cast.at[w, s, pl.ds(start, size)]
+
+    def landed_at(u, s):
+        w, start, size = units[u]
+        return landed.at[w, s - 1, pl.ds(start, size)]
+
     def first(u, s):
         return pltpu.make_async_remote_copy(
-            src_ref=cast.at[u, s],
-            dst_ref=landed.at[u, s - 1],
+            src_ref=cast_at(u, s),
+            dst_ref=landed_at(u, s),
             send_sem=send_a.at[u, s - 1],
             recv_sem=recv_a.at[u, s - 1],
             device_id={"tp": lax.rem(me + s, groups)},
@@ -347,12 +362,12 @@
         )
 
     def place(u, source):
-        w, c = units[u]
-        start = pl.multiple_of(source * rows + c * height, height)
-        return outs[w].at[expert, pl.ds(start, height)]
+        w, start, size = units[u]
+        at = pl.ds(pl.multiple_of(source * rows + start, strip), size)
+        return outs[w].at[expert, at]
 
     def second(u, s, b):
-        held = cast.at[u, 0] if s == 0 else landed.at[u, s - 1]
+        held = landed_at(u, s) if s else cast_at(u, 0)
         goal = lax.rem(me + groups - s, groups) * blocks + b
         piece = held.at[:, pl.ds(b * width, width)]
         remote = lambda: pltpu.make_async_remote_copy(
@@ -385,7 +400,7 @@
 
     def arrived(u, source):
         pltpu.make_async_copy(
-            cast.at[u, 0, :, pl.ds(0, width)], place(u, source), recv_b.at[u, source]
+            cast_at(u, 0).at[:, pl.ds(0, width)], place(u, source), recv_b.at[u, source]
         ).wait()
 
     def pack(j):
@@ -425,7 +440,7 @@
         lax.fori_loop(0, groups, one, 0)
 
     def lower(start, size):
-        at = pl.ds(pl.multiple_of(start, size), size)
+        at = pl.ds(pl.multiple_of(start, strip), size)
         partial[at, :] = lax.dot_general(
             down_w[at, :], act[...], (((1,), (1,)), ((), ())), preferred_element_type=jnp.float32
         ).astype(jnp.bfloat16)
@@ -440,13 +455,17 @@
     def level_at(d):
         return lax.rem(level // 2 + d // 2, 2) * 2 + lax.rem(level + d, 2)
 
+    lasts = [u for u in range(len(units)) if units[u][0] == 2]
+    chunks = len(lasts)
+
     def span(c):
-        return pl.ds(c * height, height)
+        return pl.ds(*units[lasts[c]][1:])
 
     def across(j, d, c):
-        start = (level_at(d) * 2 + 1 - side) * rows + c * height
+        start, size = units[lasts[c]][1:]
+        start = (level_at(d) * 2 + 1 - side) * rows + start
         return pltpu.make_async_remote_copy(
-            src_ref=partial.at[pl.ds(pl.multiple_of(start, height), height)],
+            src_ref=partial.at[pl.ds(pl.multiple_of(start, strip), size)],
             dst_ref=pair.at[j, d, span(c)],
             send_sem=send_c.at[j, d, c],
             recv_sem=recv_c.at[j, d, c],
@@ -493,18 +512,19 @@
         )
 
     def sum_into(j, d, c, target, others):
+        start, size = units[lasts[c]][1:]
         base = (level_at(d) * 2 + side) * rows
 
         def add(i, carry):
-            at = pl.ds(pl.multiple_of(c * height + i * strip, strip), strip)
-            mine = pl.ds(pl.multiple_of(base + c * height + i * strip, strip), strip)
+            at = pl.ds(pl.multiple_of(start + i * strip, strip), strip)
+            mine = pl.ds(pl.multiple_of(base + start + i * strip, strip), strip)
             value = partial[mine, :].astype(jnp.float32) + pair[j, d, at, :].astype(jnp.float32)
             for other in others:
                 value = value + other[at, :].astype(jnp.float32)
             target[at, :] = value.astype(jnp.bfloat16)
             return carry
 
-        lax.fori_loop(0, height // strip, add, 0)
+        lax.fori_loop(0, size // strip, add, 0)
 
     def to_level(j, d, c):
         across(j, d, c).wait_recv()
@@ -559,10 +579,11 @@
         for c in range(chunks):
             cross_over(0, c)
 
-    tasks = {0: after_0, 1: after_1, 2: after_2, 3: after_3, 4: after_4}
+    tasks = {1: after_0, 2: after_1, 3: after_2, 4: after_3, 5: after_4}
+    held_unit = len(units) - 1
 
     for n, (u, s) in enumerate(jobs):
-        w, c = units[u]
+        w, start, size = units[u]
         load(n).wait()
         slot = n % SLOTS
 
@@ -570,16 +591,18 @@
             at = pl.ds(pl.multiple_of(i * strip, strip), strip)
             value = stage[slot, at, :]
             if w < 2:
-                gain = gain_ref[pl.ds(pl.multiple_of(c * height + i * strip, strip), strip), :]
+                gain = gain_ref[pl.ds(pl.multiple_of(start + i * strip, strip), strip), :]
                 value = value * gain
-            cast[u, s, at, :] = value.astype(jnp.bfloat16)
+            to = pl.ds(pl.multiple_of(start + i * strip, strip), strip)
+            cast[w, s, to, :] = value.astype(jnp.bfloat16)
             return carry
 
-        lax.fori_loop(0, height // strip, convert, 0)
+        lax.fori_loop(0, size // strip, convert, 0)
         if n + SLOTS < len(jobs):
             load(n + SLOTS).start()
         if s == 0:
-            pass_on(u, 0)
+            if u != held_unit:
+                pass_on(u, 0)
         else:
             first(u, s).start()
         if n + 1 == len(jobs) or jobs[n + 1][0] != u:
@@ -587,39 +610,41 @@
                 forward(u - 1)
             if u in tasks:
                 tasks[u]()
-    forward(len(units) - 1)
     pack(1)
-    for c in range(chunks):
-        settle_sum(0, c)
-        for d in range(stack):
-            across(0, d, c).wait_send()
     for w in range(2):
         keep(w).wait()
-        for c in range(chunks):
-            for source in range(row_groups):
-                arrived(w * chunks + c, source)
+        for u in range(len(units)):
+            if units[u][0] == w:
+                for source in range(row_groups):
+                    arrived(u, source)
         fetch(w, expert).start()
     for w in range(2):
         fetch(w, expert).wait()
     hidden()
     keep(2).wait()
+    for c in range(chunks):
+        settle_sum(0, c)
+        for d in range(stack):
+            across(0, d, c).wait_send()
 
     def piece(d, i, c):
         source = level_at(d) * 2 + lax.rem(side + 1 + i, 2)
-        at = pl.ds(pl.multiple_of(source * rows + c * height, height), height)
+        start, size = units[lasts[c]][1:]
+        at = pl.ds(pl.multiple_of(source * rows + start, strip), size)
         copy = pltpu.make_async_copy(outs[2].at[expert, at], down_w.at[at], raw_sem.at[i])
         return source, copy
 
     def level_product(d, c):
         for i in range(2):
             source, copy = piece(d, i, c)
-            arrived(2 * chunks + c, source)
+            arrived(lasts[c], source)
             copy.start()
         for i in range(2):
             piece(d, i, c)[1].wait()
 
         def one(i, carry):
-            lower((level_at(d) * 2 + lax.rem(side + 1 + i, 2)) * rows + c * height, height)
+            start, size = units[lasts[c]][1:]
+            lower((level_at(d) * 2 + lax.rem(side + 1 + i, 2)) * rows + start, size)
             return carry
 
         lax.fori_loop(0, 2, one, 0)
@@ -627,15 +652,13 @@
 
     for c in range(chunks):
         for d in range(stack):
-            if c and d == 2:
-                to_level(1, 2, c - 1)
-                to_level(1, 1, c - 1)
             level_product(d, c)
-        if c:
-            cross_over(1, c - 1)
-    to_level(1, 2, chunks - 1)
-    to_level(1, 1, chunks - 1)
-    cross_over(1, chunks - 1)
+        to_level(1, 2, c)
+        to_level(1, 1, c)
+        if c == 0:
+            pass_on(held_unit, 0)
+            forward(held_unit)
+        cross_over(1, c)
     for c in range(chunks):
         settle_sum(1, c)
     for c in range(chunks):
@@ -670,9 +693,13 @@
     tokens = spots.shape[2]
     capacity = tokens // 2
     slots = groups * capacity
-    chunks = 2
-    units = 3 * chunks
-    height = rows // chunks
+    eighth = rows // 8
+    plan = [(0, 0, eighth), (0, eighth, 3 * eighth), (0, 4 * eighth, 4 * eighth)]
+    plan += [(1, 0, 4 * eighth), (1, 4 * eighth, 4 * eighth)]
+    plan += [(2, 0, 4 * eighth), (2, 4 * eighth, 2 * eighth), (2, 6 * eighth, 2 * eighth)]
+    units = len(plan)
+    chunks = 3
+    height = 4 * eighth
     stack = row_groups // 2
     out = jax.ShapeDtypeStruct((experts // groups, model_width, width), jnp.bfloat16)
     hbm = pl.BlockSpec(memory_space=pl.ANY)
@@ -681,7 +708,7 @@
     weight = pltpu.VMEM((model_width, width), jnp.bfloat16)
     dma = lambda *shape: pltpu.SemaphoreType.DMA(shape)
     return pl.pallas_call(
-        functools.partial(serve_kernel, groups, row_groups, expert, chunks),
+        functools.partial(serve_kernel, groups, row_groups, expert, plan),
         out_shape=(
             out, out, out,
             jax.ShapeDtypeStruct((groups, 2, rows, capacity), jnp.bfloat16),
@@ -690,8 +717,8 @@
         out_specs=(hbm,) * 4,
         scratch_shapes=[
             pltpu.VMEM((SLOTS, height, columns), jnp.float32),
-            pltpu.VMEM((units, groups, height, columns), jnp.bfloat16),
-            pltpu.VMEM((units, groups - 1, height, columns), jnp.bfloat16),
+            pltpu.VMEM((3, groups, rows, columns), jnp.bfloat16),
+            pltpu.VMEM((3, groups - 1, rows, columns), jnp.bfloat16),
             pltpu.VMEM((tokens, model_width), jnp.bfloat16),
             pltpu.VMEM((slots, model_width), jnp.bfloat16),
             weight, weight, weight,
@@ -745,28 +772,26 @@
     tokens, features = out_ref.shape
     groups, count, _, capacity = back_ref.shape
     logits = logit_ref[...]
-    scores = [logits[:, k : k + 1] for k in range(2)]
+    scores = [logits[k : k + 1, :] for k in range(2)]
     largest = jnp.maximum(scores[0], scores[1])
     powers = [jnp.exp(score - largest) for score in scores]
     whole = powers[0] + powers[1]
     slots = slot_ref[...]
-    value = jnp.zeros((tokens, features), jnp.float32)
+    value = jnp.zeros((features, tokens), jnp.float32)
     done = 0
     for e in range(groups * count):
         block = back_ref[e // count, e % count]
-        names = lax.broadcasted_iota(jnp.int32, (tokens, capacity), 1) + e * capacity
+        names = lax.broadcasted_iota(jnp.int32, (capacity, tokens), 0) + e * capacity
         for k in range(2):
-            table = jnp.where(names == slots[:, k : k + 1], 1.0, 0.0).astype(jnp.bfloat16)
-            picked = lax.dot_general(
-                table, block, (((1,), (1,)), ((), ())), preferred_element_type=jnp.float32
-            )
+            table = jnp.where(names == slots[k : k + 1, :], 1.0, 0.0).astype(jnp.bfloat16)
+            picked = jnp.dot(block, table, preferred_element_type=jnp.float32)
             value = value + picked * (powers[k] / whole)
         until = (e + 1) * len(pieces) // (groups * count)
         for n in range(done, until):
             load(n).wait()
             store(n).start()
         done = until
-    out_ref[...] = value.astype(jnp.bfloat16)
+    out_ref[...] = jnp.transpose(value).astype(jnp.bfloat16)
     for n in range(len(pieces)):
         store(n).wait()
 
@@ -781,7 +806,7 @@
     return pl.pallas_call(
         functools.partial(finish_kernel, parts),
         out_shape=(
-            same, same, same, jax.ShapeDtypeStruct((slots.shape[0], features), jnp.bfloat16)
+            same, same, same, jax.ShapeDtypeStruct((slots.shape[1], features), jnp.bfloat16)
         ),
         in_specs=[hbm, hbm, hbm, vmem, vmem, vmem],
         out_specs=(hbm, hbm, hbm, vmem),
@@ -792,7 +817,7 @@
         ],
         compiler_params=pltpu.CompilerParams(vmem_limit_bytes=56 * 1024 * 1024),
         cost_estimate=pl.CostEstimate(
-            flops=4 * slots.shape[0] * back.size, bytes_accessed=12 * gate.size, transcendentals=0
+            flops=4 * slots.shape[1] * back.size, bytes_accessed=12 * gate.size, transcendentals=0
         ),
     )(gate, up, down, back, slots, logits)
 
@@ -819,7 +844,7 @@
     gate, up, down, ordered = serve(
         gain, gate_master, up_master, down_master, everything, spots, firsts, 1, 2
     )
-    return finish(gate, up, down, ordered, slot_ids, route_logits, pieces)
+    return finish(gate, up, down, ordered, slot_ids.T, route_logits.T, pieces)
 
 
 def arrange(weights, groups, row_groups):

time: 637 us -> 628 us (0.986)
  Pallas kernels: 629 us -> 621 us
    pallas_call x1, Pallas kernels: 361 us -> 353 us  [serve(): pl.pallas_call(functools.partial(serve_kernel, groups, row_groups, expert...]
where the time goes in v3:
time: 628 us; the launch traced here: 627 us
  Pallas kernels  621 us (99%)
    pallas_call x1, Pallas kernels, serve(): pl.pallas_call(functools.partial(serve_kernel, groups, row_groups, expert...  353 us
    pallas_call x1, Pallas kernels, exchange(): pl.pallas_call(functools.partial(exchange_kernel, groups, row_groups, exp...  250 us
    pallas_call x1, Pallas kernels, finish(): pl.pallas_call(functools.partial(finish_kernel, parts), out_shape=(same,...  17.2 us

profile of v3, /device:TPU:0, one launch (start us, length us, event | category | flops | bytes accessed | tf_op | source)
XLA Modules:
  0.0 626.9 jit_solution(13229661218854203055)
XLA Ops:
  0.6 0.7 fusion.1
  1.3 0.2 fusion
  1.6 0.7 select_reduce_fusion
  2.3 0.6 reshape.13.spot_ref
  2.9 1.3 add_bitcast_fusion.slot_ref
  4.2 1.5 copy.18.gain_ref
  5.7 250.3 %shard_map.102 = (bf16[2048,896]{1,0:T(8,128)(2,1)}, bf16[2048,896]{1,0:T(8,128)(2,1)}, bf16[2048,896]{1,0:T(8,128)(2,1)}, bf16[8,4,512,256]{3,2,1,0:T(8,128)(2,1)}, f32[4,2,512]{2,1,0:T(2,128)}) custom-call(f32[256,1]{1,0:T(8,128)} %copy.18.gain_ref, f32[8,256,1792]{2,1,0:T(8,128)} %gate_ref.3, f32[8,256,1792]{2,1,0:T(8,128)} %up_ref.3, ...), custom_call_target="tpu_custom_call" | custom-call | flops 458752 | bytes 352321536 | tf_op jit(solution)/shard_map/pallas_call | solution.py:263
  256.0 353.5 %shard_map.103 = (bf16[2,2048,896]{2,1,0:T(8,128)(2,1)}, bf16[2,2048,896]{2,1,0:T(8,128)(2,1)}, bf16[2,2048,896]{2,1,0:T(8,128)(2,1)}, bf16[4,2,256,256]{3,2,1,0:T(8,128)(2,1)}) custom-call(f32[256,1]{1,0:T(8,128)} %copy.18.gain_ref, f32[8,256,1792]{2,1,0:T(8,128)} %gate_ref.3, f32[8,256,1792]{2,1,0:T(8,128)} %up_ref.3, f32[8,256,1792]{2,1,0:T(8,128)} %down_ref.3, ...), custom_call_target="tpu_custom_call" | custom-call | flops 22548578304 | bytes 352321536 | tf_op jit(solution)/shard_map/pallas_call | solution.py:710
  609.5 17.2 %shard_map.104 = (bf16[2,2048,896]{2,1,0:T(8,128)(2,1)}, bf16[2,2048,896]{2,1,0:T(8,128)(2,1)}, bf16[2,2048,896]{2,1,0:T(8,128)(2,1)}, bf16[512,256]{1,0:T(8,128)(2,1)}) custom-call(bf16[2,2048,896]{2,1,0:T(8,128)(2,1)} %get-tuple-element.18.gate_ref, bf16[2,2048,896]{2,1,0:T(8,128)(2,1)} %get-tuple-element.19.up_ref, ...), custom_call_target="tpu_custom_call" | custom-call | flops 1073741824 | bytes 44040192 | tf_op jit(solution)/shard_map/pallas_call | solution.py:806
  (1 shorter events, 0.0 us)

commit v4 on v3

--- a/solution.py
+++ b/solution.py
@@ -696,7 +696,7 @@
     eighth = rows // 8
     plan = [(0, 0, eighth), (0, eighth, 3 * eighth), (0, 4 * eighth, 4 * eighth)]
     plan += [(1, 0, 4 * eighth), (1, 4 * eighth, 4 * eighth)]
-    plan += [(2, 0, 4 * eighth), (2, 4 * eighth, 2 * eighth), (2, 6 * eighth, 2 * eighth)]
+    plan += [(2, 0, 3 * eighth), (2, 3 * eighth, 3 * eighth), (2, 6 * eighth, 2 * eighth)]
     units = len(plan)
     chunks = 3
     height = 4 * eighth

time: 628 us -> 624 us (level)
  no operation moved by 1% of the time
where the time goes in v4:
time: 624 us; the launch traced here: 623 us
  Pallas kernels  617 us (99%)
    pallas_call x1, Pallas kernels, serve(): pl.pallas_call(functools.partial(serve_kernel, groups, row_groups, expert...  349 us
    pallas_call x1, Pallas kernels, exchange(): pl.pallas_call(functools.partial(exchange_kernel, groups, row_groups, exp...  250 us
    pallas_call x1, Pallas kernels, finish(): pl.pallas_call(functools.partial(finish_kernel, parts), out_shape=(same,...  17.2 us

profile of v4, /device:TPU:0, one launch (start us, length us, event | category | flops | bytes accessed | tf_op | source)
XLA Modules:
  0.0 622.9 jit_solution(914810412310462776)
XLA Ops:
  0.6 0.7 fusion.1
  1.3 0.2 fusion
  1.6 0.7 select_reduce_fusion
  2.3 0.6 reshape.13.spot_ref
  2.9 1.3 add_bitcast_fusion.slot_ref
  4.2 1.5 copy.18.gain_ref
  5.7 250.3 %shard_map.102 = (bf16[2048,896]{1,0:T(8,128)(2,1)}, bf16[2048,896]{1,0:T(8,128)(2,1)}, bf16[2048,896]{1,0:T(8,128)(2,1)}, bf16[8,4,512,256]{3,2,1,0:T(8,128)(2,1)}, f32[4,2,512]{2,1,0:T(2,128)}) custom-call(f32[256,1]{1,0:T(8,128)} %copy.18.gain_ref, f32[8,256,1792]{2,1,0:T(8,128)} %gate_ref.3, f32[8,256,1792]{2,1,0:T(8,128)} %up_ref.3, ...), custom_call_target="tpu_custom_call" | custom-call | flops 458752 | bytes 352321536 | tf_op jit(solution)/shard_map/pallas_call | solution.py:263
  256.0 349.5 %shard_map.103 = (bf16[2,2048,896]{2,1,0:T(8,128)(2,1)}, bf16[2,2048,896]{2,1,0:T(8,128)(2,1)}, bf16[2,2048,896]{2,1,0:T(8,128)(2,1)}, bf16[4,2,256,256]{3,2,1,0:T(8,128)(2,1)}) custom-call(f32[256,1]{1,0:T(8,128)} %copy.18.gain_ref, f32[8,256,1792]{2,1,0:T(8,128)} %gate_ref.3, f32[8,256,1792]{2,1,0:T(8,128)} %up_ref.3, f32[8,256,1792]{2,1,0:T(8,128)} %down_ref.3, ...), custom_call_target="tpu_custom_call" | custom-call | flops 22548578304 | bytes 352321536 | tf_op jit(solution)/shard_map/pallas_call | solution.py:710
  605.5 17.2 %shard_map.104 = (bf16[2,2048,896]{2,1,0:T(8,128)(2,1)}, bf16[2,2048,896]{2,1,0:T(8,128)(2,1)}, bf16[2,2048,896]{2,1,0:T(8,128)(2,1)}, bf16[512,256]{1,0:T(8,128)(2,1)}) custom-call(bf16[2,2048,896]{2,1,0:T(8,128)(2,1)} %get-tuple-element.18.gate_ref, bf16[2,2048,896]{2,1,0:T(8,128)(2,1)} %get-tuple-element.19.up_ref, ...), custom_call_target="tpu_custom_call" | custom-call | flops 1073741824 | bytes 44040192 | tf_op jit(solution)/shard_map/pallas_call | solution.py:806
  (1 shorter events, 0.0 us)
